TPU v7x, 32 devices: a whole 2x2x4 slice. The times are simulated.
32 devices in a mesh: sp: 16 (over z, y, x), tp: 2 (over core).
Axes of the slice: x: 2, y: 2, z: 4, core: 2. Of those that a mesh axis runs over, the one named last changes fastest.
Arguments:
- stream_in: bfloat16 [2048, 2048], P(('sp', 'tp')), may hold values from -6 to 6
- query_rows: bfloat16 [2048, 2048], P('sp', 'tp'), may hold values from -6 to 6
- key_rows: bfloat16 [2048, 2048], P('sp', 'tp'), may hold values from -6 to 6
- value_rows: bfloat16 [2048, 2048], P('sp', 'tp'), may hold values from -6 to 6
- removal_key: bfloat16 [2048, 2048], P('sp', 'tp'), may hold values from -6 to 6
- learn_pre: bfloat16 [2048, 2048], P('sp', 'tp'), may hold values from -12 to 4
- log_rate: float32 [2048, 2048], P('sp', 'tp'), may hold values from -14 to 0
- norm_gain: bfloat16 [2048], P('tp'), may hold values from 0.099609375 to 1.8984375
- out_weight: bfloat16 [2048, 2048], replicated, may hold values from -0.125 to 0.125
- ffn_gain: bfloat16 [2048], replicated, may hold values from 0.099609375 to 1.8984375
- routes: int32 [2048, 2], P(('sp', 'tp')), may hold values from 0 to 7, all different within a row; in each aligned block of 64 rows (0 to 63, 64 to 127, ...) at most 32 rows name the same one
- route_weight: float32 [2048, 2], P(('sp', 'tp')), may hold values from 0.1 to 1
- expert_gate: bfloat16 [16, 2048, 1792], P('sp', None, 'tp'), may hold values from -0.125 to 0.125
- expert_up: bfloat16 [16, 2048, 1792], P('sp', None, 'tp'), may hold values from -0.125 to 0.125
- expert_down: bfloat16 [16, 1792, 2048], P('sp', 'tp'), may hold values from -0.09375 to 0.09375
Outputs:
- layer_out: bfloat16 [2048, 2048], P(('sp', 'tp'))
Inputs may be any that keep to these rules, and one draw needn't show every extreme that they name: `routes`: in each aligned block of 64 rows (the rows of one device after the mixer) no expert is named by more than 32 rows, a bound that some expert reaches in some or all blocks; the experts of one row differ.
All inputs are finite; a program needn't handle non-finite values.
Results may differ from a plain program's by a relative error of at most 0.0065.
Values may be sent and summed in bfloat16 or wider, within the bound.
A program may use at most 192 MiB of HBM per device.

v0:
```python
import jax
import jax.numpy as jnp
from jax import lax
from jax.sharding import PartitionSpec as P

HEAD = 64
TOPK = 2
SPAN = 16


HIGH = lax.Precision.HIGHEST
GROUP_EPS = 0.00064
NORM_EPS = 1e-06
UNIT_EPS = 1e-06


def carried_in(array, axis, combine, identity):
    length, place = (lax.axis_size(axis), lax.axis_index(axis))
    everything = jax.tree.map(lambda part: lax.all_gather(part, axis), array)
    start = jax.tree.map(
        lambda part, zero: jnp.broadcast_to(jnp.asarray(zero, part.dtype), part.shape),
        array,
        identity,
    )

    def lap(k, before):
        reached = k < place
        new = combine(before, jax.tree.map(lambda part: part[k], everything))
        return jax.tree.map(lambda a, b: jnp.where(reached, a, b), new, before)

    return lax.fori_loop(0, length, lap, start)


def from_partner(array, axis, bit):
    return lax.ppermute(array, axis, [(i, i ^ 1 << bit) for i in range(lax.axis_size(axis))])


def block_terms(queries, key_vals, values, unit_key, pull_key, log_decay):
    span = queries.shape[2]
    head_size = queries.shape[3]
    cumul = jnp.cumsum(log_decay, axis=2)
    before = cumul - log_decay
    position = jnp.arange(span, dtype=jnp.int32)
    strict = (position[:, None] > position[None, :]).astype(jnp.float32)
    upto = (position[:, None] >= position[None, :]).astype(jnp.float32)
    fade_prev = (
        jnp.exp(jnp.minimum(before[:, :, :, None, :] - cumul[:, :, None, :, :], 0.0))
        * strict[:, :, None]
    )
    fade_now = (
        jnp.exp(jnp.minimum(cumul[:, :, :, None, :] - cumul[:, :, None, :, :], 0.0))
        * upto[:, :, None]
    )
    mix_pull = jnp.einsum("bhtk,bhtjk,bhjk->bhtj", unit_key, fade_prev, pull_key, precision=HIGH)
    mix_key = jnp.einsum("bhtk,bhtjk,bhjk->bhtj", unit_key, fade_prev, key_vals, precision=HIGH)
    read_key = jnp.einsum("bhtk,bhtjk,bhjk->bhtj", queries, fade_now, key_vals, precision=HIGH)
    read_pull = jnp.einsum("bhtk,bhtjk,bhjk->bhtj", queries, fade_now, pull_key, precision=HIGH)
    system = mix_pull + jnp.eye(span, dtype=jnp.float32)
    starts = unit_key * jnp.exp(before)
    sources = jnp.concatenate((jnp.matmul(mix_key, values, precision=HIGH), starts), axis=-1)
    solved = lax.linalg.triangular_solve(
        system, sources, left_side=True, lower=True, unit_diagonal=True
    )
    removed = solved[..., :head_size]
    weights = solved[..., head_size:]
    local_read = jnp.matmul(read_key, values, precision=HIGH) - jnp.matmul(
        read_pull, removed, precision=HIGH
    )
    carry_read = queries * jnp.exp(cumul) - jnp.matmul(read_pull, weights, precision=HIGH)
    tail = jnp.exp(cumul[:, :, -1:, :] - cumul)
    key_tail = key_vals * tail
    pull_tail = pull_key * tail
    block_state = jnp.einsum("bhjv,bhjk->bhvk", values, key_tail, precision=HIGH) - jnp.einsum(
        "bhjv,bhjk->bhvk", removed, pull_tail, precision=HIGH
    )
    last_decay = jnp.exp(cumul[:, :, -1, :])
    block_map = last_decay[..., :, None] * jnp.eye(head_size, dtype=jnp.float32) - jnp.einsum(
        "bhjk,bhjl->bhkl", weights, pull_tail, precision=HIGH
    )
    return (block_map, block_state, local_read, carry_read)


def across_blocks(carry, block):
    prefix_map, prefix_state = carry
    block_map, block_state = block
    new_map = jnp.matmul(prefix_map, block_map, precision=HIGH)
    new_state = jnp.matmul(prefix_state, block_map, precision=HIGH) + block_state
    return ((new_map, new_state), (prefix_map, prefix_state))


def compose(earlier, later):
    joined_map = jnp.matmul(earlier[0], later[0], precision=HIGH)
    joined_state = jnp.matmul(earlier[1], later[0], precision=HIGH) + later[1]
    return (joined_map, joined_state)


def local(
    stream_in,
    query_rows,
    key_rows,
    value_rows,
    removal_key,
    learn_pre,
    log_rate,
    norm_gain,
    out_weight,
    ffn_gain,
    routes,
    route_weight,
    expert_gate,
    expert_up,
    expert_down,
):
    tokens_dev = query_rows.shape[0]
    heads_dev = query_rows.shape[1] // HEAD
    blocks = tokens_dev // SPAN

    def blocked(array):
        shaped = array.astype(jnp.float32).reshape(blocks, SPAN, heads_dev, HEAD)
        return shaped.transpose(0, 2, 1, 3)

    removal = blocked(removal_key)
    unit_key = removal / jnp.sqrt(jnp.sum(removal * removal, axis=-1, keepdims=True) + UNIT_EPS)
    pull_key = unit_key * jax.nn.sigmoid(blocked(learn_pre))
    log_decay = -jnp.exp(blocked(log_rate))
    identity = jnp.broadcast_to(jnp.eye(HEAD, dtype=jnp.float32), (heads_dev, HEAD, HEAD))
    nothing = jnp.zeros((heads_dev, HEAD, HEAD), jnp.float32)
    block_map, block_state, local_read, carry_read = block_terms(
        blocked(query_rows), blocked(key_rows), blocked(value_rows), unit_key, pull_key, log_decay
    )
    (device_map, device_state), (prefix_map, prefix_state) = lax.scan(
        across_blocks, (identity, nothing), (block_map, block_state)
    )
    entering = carried_in((device_map, device_state), "sp", compose, (identity, nothing))
    block_start = jnp.matmul(entering[1][None], prefix_map, precision=HIGH) + prefix_state
    mixed = local_read + jnp.einsum("bhvk,bhtk->bhtv", block_start, carry_read, precision=HIGH)
    mixed = mixed.transpose(0, 2, 1, 3).reshape(tokens_dev, heads_dev, HEAD)
    centred = mixed - jnp.mean(mixed, axis=-1, keepdims=True)
    variance = jnp.mean(centred * centred, axis=-1, keepdims=True)
    normed = (centred * lax.rsqrt(variance + GROUP_EPS)).reshape(tokens_dev, heads_dev * HEAD)
    normed = (normed * norm_gain.astype(jnp.float32)).astype(jnp.bfloat16)
    gathered = lax.all_to_all(normed, "tp", split_axis=0, concat_axis=1, tiled=True)
    attended = stream_in.astype(jnp.float32) + jnp.dot(
        gathered, out_weight, preferred_element_type=jnp.float32
    )
    scaling = lax.rsqrt(jnp.mean(attended * attended, axis=-1, keepdims=True) + NORM_EPS)
    ffn_in = (attended * scaling * ffn_gain.astype(jnp.float32)).astype(jnp.bfloat16)
    half_rows = attended.shape[0]
    width = attended.shape[1]
    experts = lax.axis_size("sp") // 2
    peers = lax.axis_size("sp") * lax.axis_size("tp")
    capacity = 2 * TOPK * half_rows // experts
    pairs = half_rows * TOPK
    expert_ids = routes.reshape(pairs)
    one_hot = (expert_ids[:, None] == jnp.arange(experts, dtype=jnp.int32)[None, :]).astype(
        jnp.int32
    )
    slot_index = jnp.sum(jnp.cumsum(one_hot, axis=0) * one_hot, axis=1) - 1
    send_index = expert_ids * capacity + slot_index
    send_map = (
        jnp.arange(experts * capacity, dtype=jnp.int32)[:, None] == send_index[None, :]
    ).astype(jnp.bfloat16)
    send_map = jnp.sum(send_map.reshape(experts * capacity, half_rows, TOPK), axis=2)
    dispatched = jnp.dot(send_map, ffn_in, preferred_element_type=jnp.float32).astype(jnp.bfloat16)
    quarters = lax.all_to_all(dispatched, ("sp", "tp"), split_axis=0, concat_axis=0, tiled=True)
    quarters = quarters.reshape(peers, capacity // 4, width)
    chip_pair = lax.all_gather(quarters, "tp", axis=1, tiled=True)
    partner = from_partner(chip_pair, "sp", 0)
    low_first = jnp.concatenate((chip_pair, partner), axis=1)
    high_first = jnp.concatenate((partner, chip_pair), axis=1)
    routed = jnp.where(lax.axis_index("sp") % 2 == 0, low_first, high_first).reshape(
        peers * capacity, width
    )
    gate_act = jnp.dot(routed, expert_gate[0], preferred_element_type=jnp.float32)
    up_act = jnp.dot(routed, expert_up[0], preferred_element_type=jnp.float32)
    hidden = (jax.nn.silu(gate_act) * up_act).astype(jnp.bfloat16)
    partial_out = jnp.dot(hidden, expert_down[0], preferred_element_type=jnp.float32).astype(
        jnp.bfloat16
    )
    partial_out = partial_out.reshape(peers, capacity, width)
    pair_bit = lax.axis_index("sp") % 2
    half_width = width // 2
    kept_half = lax.dynamic_slice_in_dim(partial_out, pair_bit * half_width, half_width, 2)
    sent_half = lax.dynamic_slice_in_dim(partial_out, (1 - pair_bit) * half_width, half_width, 2)
    partner_half = from_partner(sent_half, "sp", 0)
    pair_sum = kept_half.astype(jnp.float32) + partner_half.astype(jnp.float32)
    expert_out = lax.psum_scatter(
        pair_sum.astype(jnp.bfloat16), "tp", scatter_dimension=2, tiled=True
    )
    returned = lax.all_to_all(expert_out, ("sp", "tp"), split_axis=0, concat_axis=2, tiled=True)
    returned = returned.reshape(capacity * experts, width)
    back_index = slot_index * experts + expert_ids
    back_map = (
        back_index[:, None] == jnp.arange(capacity * experts, dtype=jnp.int32)[None, :]
    ).astype(jnp.bfloat16)
    picked = jnp.dot(back_map, returned, preferred_element_type=jnp.float32).reshape(
        half_rows, TOPK, width
    )
    mixture = jnp.sum(picked * route_weight[:, :, None], axis=1)
    return (attended + mixture).astype(jnp.bfloat16)


def solution(mesh):
    placed = (
        P(("sp", "tp"), None),
        P("sp", "tp"),
        P("sp", "tp"),
        P("sp", "tp"),
        P("sp", "tp"),
        P("sp", "tp"),
        P("sp", "tp"),
        P("tp"),
        P(),
        P(),
        P(("sp", "tp"), None),
        P(("sp", "tp"), None),
        P("sp", None, "tp"),
        P("sp", None, "tp"),
        P("sp", "tp", None),
    )
    return jax.shard_map(
        local, mesh=mesh, in_specs=placed, out_specs=P(("sp", "tp"), None), check_vma=False
    )
```

profile of v0, /device:TPU:0, one launch (start us, length us, event | category | flops | bytes accessed | tf_op | source)
XLA Modules:
  0.0 860.9 jit_solution(5926493346697543820)
XLA Ops:
  8.0 5.1 fusion.69
  14.6 2.1 add_divide_fusion
  16.7 2.3 reshape.237
  19.0 2.2 reshape.238
  21.2 2.2 reshape.239
  26.7 4.1 exponential_multiply_fusion.6
  31.2 30.3 %fusion.20 = f32[8,16,16,1,16]{4,3,2,1,0:T(1,128)} fusion(f32[8,16,16,64,1]{3,4,2,1,0:T(1,128)S(1)} %bitcast.173, f32[16,16]{1,0:T(8,128)S(1)} %fusion.103, f32[8,16,16,64]{3,2,1,0:T(8,128)S(1)} %get-tuple-element.273, f32[8,16,16,64]{3,2,1,0:T(8,128)S(1)} %bitcast.184, f32[8,16,16,64]{3,2,1,0:T(8,128)S(1)} %get-tuple-element.275), kind=kOutput, calls=%fused_computation.27 | convolution fusion | flops 33554432 | bytes 2229248 | tf_op jit(solution)/shard_map/bhtk,bhtjk,bhjk->bhtj/dot_general | solution.py:55
  61.5 29.1 %fusion.22 = f32[8,16,16,1,16]{4,3,2,1,0:T(1,128)S(1)} fusion(f32[8,16,16,64,1]{3,4,2,1,0:T(1,128)S(1)} %bitcast.174, f32[16,16]{1,0:T(8,128)S(1)} %fusion.103, f32[8,16,16,64]{3,2,1,0:T(8,128)S(1)} %get-tuple-element.273, f32[8,16,16,64]{3,2,1,0:T(8,128)S(1)} %bitcast_multiply_fusion, f32[8,16,16,64]{3,2,1,0:T(8,128)S(1)} %get-tuple-element.275), kind=kOutput, calls=%fused_computation.29 | convolution fusion | flops 33554432 | bytes 2229248 | tf_op jit(solution)/shard_map/bhtk,bhtjk,bhjk->bhtj/dot_general | solution.py:54
  91.7 160.3 %custom-call.3 = f32[8,16,1,16,16]{3,4,2,1,0:T(8,128)} custom-call(f32[8,16,1,16,16]{4,3,2,1,0:T(8,128)} %add_bitcast_fusion), custom_call_target="InvertDiagBlocksLowerTriangular" | custom-call | tf_op jit(solution)/shard_map/triangular_solve | solution.py:61
  251.9 2.1 fusion.83
  254.0 4.8 fusion.71
  258.9 2.1 fusion.63
  261.0 8.4 bitcast_subtract_fusion
  269.4 9.8 %multiply_subtract_fusion = f32[8,16,64,64]{3,2,1,0:T(8,128)} fusion(f32[64,64]{1,0:T(8,128)S(1)} %fusion.101, f32[8,16,64]{2,1,0:T(8,128)S(1)} %fusion.112, f32[8,16,16,128]{3,2,1,0:T(8,128)S(1)} %fusion.63, f32[8,16,16,64]{3,2,1,0:T(8,128)S(1)} %bitcast_multiply_fusion, f32[8,16,64]{2,1,0:T(8,128)S(1)} %slice_bitcast_fusion, f32[8,16,16,64]{3,1,2,0:T(8,128)S(1)} %fusion.69), kind=kOutput, calls=%fused_computation.66 | convolution fusion | flops 101974016 | bytes 4276224 | tf_op jit(solution)/shard_map/bhjk,bhjl->bhkl/dot_general | solution.py:77
  279.3 50.6 %while.31 = (s32[]{:T(128)}, f32[16,64,64]{1,2,0:T(8,128)S(1)}, f32[16,64,64]{1,2,0:T(8,128)S(1)}, f32[8,16,64,64]{2,3,1,0:T(8,128)}, f32[8,16,64,64]{3,2,1,0:T(...) while((s32[]{:T(128)}, f32[16,64,64]{1,2,0:T(8,128)S(1)}, ...), condition=%wide.region_3.4_spmd.clone, body=%wide.region_2.3_spmd.clone.sunk | while | flops 100859904 | bytes 6293115 | solution.py:131
  279.5 2.2 fusion.144
  283.6 2.0 convolution_bitcast_fusion.4
  285.8 2.2 fusion.144
  289.9 2.0 convolution_bitcast_fusion.4
  292.1 2.2 fusion.144
  296.3 2.0 convolution_bitcast_fusion.4
  298.5 2.2 fusion.144
  304.8 2.2 fusion.144
  311.1 2.2 fusion.144
  317.4 2.2 fusion.144
  321.5 2.0 convolution_bitcast_fusion.4
  323.7 2.2 fusion.144
  327.9 2.0 convolution_bitcast_fusion.4
  333.8 17.7 %fusion.26 = f32[8,16,16,1,16]{4,3,2,1,0:T(1,128)S(1)} fusion(f32[8,16,16,64]{3,2,1,0:T(8,128)} %bitcast.185, f32[16,16]{1,0:T(8,128)S(1)} %fusion.102, f32[8,16,16,64]{3,2,1,0:T(8,128)S(1)} %copy-done.15, bf16[8,16,16,64,1]{3,2,1,0,4:T(8,128)(2,1)S(1)} %bitcast.191), kind=kOutput, calls=%fused_computation.33 | convolution fusion | flops 33554432 | bytes 1442816 | tf_op jit(solution)/shard_map/bhtk,bhtjk,bhjk->bhtj/dot_general | solution.py:56
  353.2 16.5 %fusion.24 = f32[8,16,16,1,16]{4,3,2,1,0:T(1,128)S(1)} fusion(f32[8,16,16,64]{3,2,1,0:T(8,128)S(1)} %copy-done.4, f32[16,16]{1,0:T(8,128)S(1)} %fusion.102, f32[8,16,16,64]{3,2,1,0:T(8,128)S(1)} %copy-done.15, bf16[8,16,16,64,1]{3,2,1,0,4:T(8,128)(2,1)S(1)} %bitcast.192), kind=kOutput, calls=%fused_computation.31 | convolution fusion | flops 33554432 | bytes 1442816 | tf_op jit(solution)/shard_map/bhtk,bhtjk,bhjk->bhtj/dot_general | solution.py:57
  372.3 73.9 %all-gather.8.cloned.1.call-done = f32[256,64,64]{2,1,0:T(8,128)} async-done(((f32[16,64,64]{2,1,0:T(8,128)}), f32[256,64,64]{2,1,0:T(8,128)}) %all-gather.8.cloned.1.call-update) | async-done | bytes 4194320 | tf_op jit(solution)/shard_map/all_gather | solution.py:19
  446.1 113.3 %all-gather.10.cloned.1.call-done = f32[256,64,64]{2,1,0:T(8,128)} async-done(((f32[16,64,64]{2,1,0:T(8,128)}), f32[256,64,64]{2,1,0:T(8,128)}) %all-gather.10.cloned.1.call-update) | async-done | bytes 4194320 | tf_op jit(solution)/shard_map/all_gather | solution.py:19
  559.4 54.7 %while.32 = (s32[]{:T(128)}, f32[16,64,64]{1,2,0:T(8,128)S(1)}, s32[]{:T(128)}, f32[16,16,64,64]{3,2,1,0:T(8,128)}, f32[16,16,64,64]{3,2,1,0:T(8,128)}, /*index=5*/s32[]{:T(128)}, s32[]{:T(128)}) while((s32[]{:T(128)}, f32[16,64,64]{1,2,0:T(8,128)S(1)}, s32[]{:T(128)}, f32[16,16,64,64]{3,2,1,0:T(8,128)}, ...), condition=%wide.region_5.6_spmd.clone, body=%wide.region_4.5_spmd.clone.sunk | while | flops 50593796 | bytes 3934315 | solution.py:31
  560.8 2.1 fusion.147
  564.2 2.1 fusion.147
  567.6 2.1 fusion.147
  571.0 2.1 fusion.147
  574.4 2.1 fusion.147
  577.9 2.1 fusion.147
  581.3 2.1 fusion.147
  584.7 2.1 fusion.147
  588.1 2.1 fusion.147
  591.6 2.1 fusion.147
  595.0 2.1 fusion.147
  598.4 2.1 fusion.147
  601.8 2.1 fusion.147
  605.2 2.1 fusion.147
  608.7 2.1 fusion.147
  612.1 2.1 fusion.147
  614.2 14.6 %fusion.80 = f32[16,64,8,64]{3,1,0,2:T(8,128)S(1)} fusion(f32[8,16,64,64]{2,3,1,0:T(8,128)} %get-tuple-element.142, f32[16,64,64]{1,2,0:T(8,128)S(1)} %get-tuple-element.141), kind=kOutput, calls=%fused_computation.110 | convolution fusion | flops 402653184 | bytes 4456448 | tf_op jit(solution)/shard_map/dot_general | solution.py:135
  628.8 6.6 fusion.52
  639.8 3.9 all_to_all.40
  643.8 5.1 multiply_reduce_fusion.1
  649.4 28.9 %all_to_all.41 = bf16[32,8,2048]{2,1,0:T(8,128)(2,1)} all-to-all(bf16[32,8,2048]{2,1,0:T(8,128)(2,1)S(1)} %fusion.58), channel_id=1, replica_groups=mesh['sp'=16,'tp'=2] {'sp','tp'}, dimensions={0} | all-to-all | bytes 2097152 | tf_op jit(solution)/shard_map/all_to_all | solution.py:165
  678.4 9.7 %all-gather.6.cloned.1.call-done = bf16[32,16,2048]{2,1,0:T(8,128)(2,1)} async-done(((bf16[32,8,2048]{2,1,0:T(8,128)(2,1)}), bf16[32,16,2048]{2,1,0:T(8,128)(2,1)}) %all-gather.6.cloned.1.call-update) | async-done | bytes 2097168 | tf_op jit(solution)/shard_map/all_gather | solution.py:167
  689.8 46.3 %collective-permute-done = bf16[32,16,2048]{2,1,0:T(8,128)(2,1)S(1)} collective-permute-done((bf16[32,16,2048]{2,1,0:T(8,128)(2,1)}, bf16[32,16,2048]{2,1,0:T(8,128)(2,1)S(1)}, u32[]{:S(2)}, u32[]{:S(2)}) %collective-permute-start) | collective-permute-done | bytes 2097184 | tf_op jit(solution)/shard_map/ppermute | solution.py:35
  736.1 4.2 maximum_select_fusion
  740.3 4.5 fusion.54
  744.8 4.5 fusion.56
  749.3 4.8 convolution_convert_fusion
  759.4 45.4 %collective-permute-done.1 = bf16[32,32,1024]{2,1,0:T(8,128)(2,1)S(1)} collective-permute-done((bf16[32,32,1024]{2,1,0:T(8,128)(2,1)}, bf16[32,32,1024]{2,1,0:T(8,128)(2,1)S(1)}, u32[]{:S(2)}, u32[]{:S(2)}) %collective-permute-start.1) | collective-permute-done | bytes 2097184 | tf_op jit(solution)/shard_map/ppermute | solution.py:35
  804.8 3.9 add_convert_fusion
  808.7 11.0 %reduce-scatter.2.cloned.1.call-done = bf16[32,32,512]{2,1,0:T(8,128)(2,1)} async-done(((bf16[32,32,1024]{2,1,0:T(8,128)(2,1)}), bf16[32,32,512]{2,1,0:T(8,128)(2,1)}) %reduce-scatter.2.cloned.1.call-update) | async-done | bytes 1048592 | tf_op jit(solution)/shard_map/reduce_scatter | solution.py:187
  819.7 32.1 %all_to_all.42 = bf16[32,32,512]{2,1,0:T(8,128)(2,1)S(1)} all-to-all(bf16[32,32,512]{2,1,0:T(8,128)(2,1)} %reduce-scatter.2.cloned.1.call-done), channel_id=1, replica_groups=mesh['sp'=16,'tp'=2] {'sp','tp'}, dimensions={0} | all-to-all | bytes 2097152 | tf_op jit(solution)/shard_map/all_to_all | solution.py:190
  (224 shorter events, 73.4 us)
Async XLA Ops:
  6.5 439.6 %all-gather.8.cloned.1.call-start = ((), (), s32[]{:S(2)}) async-start(), calls=%async_computation.6 | async-start | bytes 8912896 | tf_op jit(solution)/shard_map/all_gather | solution.py:19
  14.6 239.4 %copy-start.5 = (bf16[8,16,16,64]{3,2,1,0:T(8,128)(2,1)}, bf16[8,16,16,64]{3,2,1,0:T(8,128)(2,1)S(1)}, u32[]{:S(2)}) copy-start(bf16[8,16,16,64]{3,2,1,0:T(8,128)(2,1)S(1)} %reshape.231) | copy-start | bytes 786436
  26.7 4.5 copy-start.16
  26.7 4.1 copy-start.8
  30.8 30.7 %copy-start.14 = (f32[8,16,16,64]{3,2,1,0:T(8,128)}, f32[8,16,16,64]{3,2,1,0:T(8,128)S(1)}, u32[]{:S(2)}) copy-start(f32[8,16,16,64]{3,2,1,0:T(8,128)S(1)} %get-tuple-element.275) | copy-start | bytes 1572868
  31.2 238.2 %copy-start.3 = (f32[8,16,16,64]{3,2,1,0:T(8,128)}, f32[8,16,16,64]{3,2,1,0:T(8,128)S(1)}, u32[]{:S(2)}) copy-start(f32[8,16,16,64]{3,2,1,0:T(8,128)S(1)} %bitcast_multiply_fusion) | copy-start | bytes 1572868
  251.9 6.9 copy-start.10
  251.9 6.9 copy-start.17
  261.0 8.4 copy-start
  279.2 52.9 %copy-start.22 = (bf16[1024]{0:T(1024)(128)(2,1)S(1)}, bf16[1024]{0:T(1024)(128)(2,1)}, u32[]{:S(2)}) copy-start(bf16[1024]{0:T(1024)(128)(2,1)} %param.26) | copy-start | bytes 6148
  279.3 52.9 %copy-start.20 = (bf16[2048]{0:T(1024)(128)(2,1)S(1)}, bf16[2048]{0:T(1024)(128)(2,1)}, u32[]{:S(2)}) copy-start(bf16[2048]{0:T(1024)(128)(2,1)} %param.28) | copy-start | bytes 12292
  279.3 52.9 %copy-start.21 = (s32[64,2]{0,1:T(2,128)S(1)}, s32[64,2]{0,1:T(2,128)}, u32[]{:S(2)}) copy-start(s32[64,2]{0,1:T(2,128)} %param.29) | copy-start | bytes 1540
  279.3 53.8 %copy-start.19 = (bf16[128,1024]{1,0:T(8,128)(2,1)S(1)}, bf16[128,1024]{1,0:T(8,128)(2,1)}, u32[]{:S(2)}) copy-start(bf16[128,1024]{1,0:T(8,128)(2,1)} %param.20) | copy-start | bytes 786436
  329.9 3.8 copy-start.15
  331.0 228.4 %all-gather.10.cloned.1.call-start = ((), (), s32[]{:S(2)}) async-start(), calls=%async_computation.7 | async-start | bytes 8912896 | tf_op jit(solution)/shard_map/all_gather | solution.py:19
  332.1 356.0 %all-gather.6.cloned.1.call-start = ((), (), s32[]{:S(2)}) async-start(), calls=%async_computation.4 | async-start | bytes 3145728 | tf_op jit(solution)/shard_map/all_gather | solution.py:167
  333.7 17.7 %copy-start.6 = (bf16[8,16,16,64]{3,2,1,0:T(8,128)(2,1)S(1)}, bf16[8,16,16,64]{3,2,1,0:T(8,128)(2,1)}, u32[]{:S(2)}) copy-start(bf16[8,16,16,64]{3,2,1,0:T(8,128)(2,1)} %copy-done.5) | copy-start | bytes 786436
  333.7 19.4 %copy-start.4 = (f32[8,16,16,64]{3,2,1,0:T(8,128)S(1)}, f32[8,16,16,64]{3,2,1,0:T(8,128)}, u32[]{:S(2)}) copy-start(f32[8,16,16,64]{3,2,1,0:T(8,128)} %copy-done.3) | copy-start | bytes 1572868
  353.2 17.5 %copy-start.1 = (f32[8,16,16,128]{3,2,1,0:T(8,128)S(1)}, f32[8,16,16,128]{3,2,1,0:T(8,128)}, u32[]{:S(2)}) copy-start(f32[8,16,16,128]{3,2,1,0:T(8,128)} %copy-done) | copy-start | bytes 3145732
  369.7 1.0 copy-start.12
  614.2 14.6 %copy-start.9 = (f32[8,16,64,64]{3,2,1,0:T(8,128)S(1)}, f32[8,16,64,64]{3,2,1,0:T(8,128)}, u32[]{:S(2)}) copy-start(f32[8,16,64,64]{3,2,1,0:T(8,128)} %get-tuple-element.143) | copy-start | bytes 6291460
  628.8 6.6 copy-start.2
  628.8 6.6 copy-start.11
  628.8 6.6 copy-start.13
  638.3 5.5 copy-start.18
  678.3 141.4 %reduce-scatter.2.cloned.1.call-start = ((), (), s32[]{:S(2)}) async-start(), calls=%async_computation.5 | async-start | bytes 3145728 | tf_op jit(solution)/shard_map/reduce_scatter | solution.py:187
  688.0 48.0 %collective-permute-start = (bf16[32,16,2048]{2,1,0:T(8,128)(2,1)}, bf16[32,16,2048]{2,1,0:T(8,128)(2,1)S(1)}, u32[]{:S(2)}, u32[]{:S(2)}) collective-permute-start(bf16[32,16,2048]{2,1,0:T(8,128)(2,1)} %all-gather.6.cloned.1.call-done), channel_id=1, source_target_pairs={{0,2},{2,0},{4,6},{6,4},{8,10},{10,8},{12,14},{14,12},{16,18},{18,... | collective-permute-start | bytes 6291464 | tf_op jit(solution)/shard_map/ppermute | solution.py:35
  689.8 50.5 %copy-start.24 = (bf16[1,2048,896]{2,1,0:T(8,128)(2,1)S(1)}, bf16[1,2048,896]{2,1,0:T(8,128)(2,1)}, u32[]{:S(2)}) copy-start(bf16[1,2048,896]{2,1,0:T(8,128)(2,1)} %param.32) | copy-start | bytes 11010052
  740.3 4.5 copy-start.25
  744.8 4.5 copy-start.26
  754.1 2.0 copy-start.7
  757.6 47.2 %collective-permute-start.1 = (bf16[32,32,1024]{2,1,0:T(8,128)(2,1)}, bf16[32,32,1024]{2,1,0:T(8,128)(2,1)S(1)}, u32[]{:S(2)}, u32[]{:S(2)}) collective-permute-start(bf16[32,32,1024]{2,1,0:T(8,128)(2,1)} %constant_dynamic-slice_fusion.1), channel_id=1, source_target_pairs={{0,2},{2,0},{4,6},{6,4},{8,10},{10,8},{12,14},{14,12},{16,18},{18,... | collective-permute-start | bytes 6291464 | tf_op jit(solution)/shard_map/ppermute | solution.py:35
  808.7 44.3 %copy-start.23 = (f32[64,2]{0,1:T(2,128)S(1)}, f32[64,2]{0,1:T(2,128)}, u32[]{:S(2)}) copy-start(f32[64,2]{0,1:T(2,128)} %param.30) | copy-start | bytes 1540
Sparse Core Ops, SparseCore 0:
  331.1 115.0 all-gather.7
  448.9 110.4 all-gather.9
  678.4 9.5 all-gather.5
  808.9 10.7 reduce-scatter.1
where the time goes:
time: 868 us; the launch traced here: 861 us
  waiting for transfers between devices  300 us (35%)
  matrix products  233 us (27%)
  other arithmetic  186 us (21%)
  blocking collectives  64.9 us (7%)
  local copies, waits for them, and re-layouts  57.9 us (7%)
  between operations  14 us (2%)
    all_gather x2, waiting for transfers between devices, carried_in(): everything = jax.tree.map(lambda part: lax.all_gather(part, axis), array)  187 us
    another operation x5, other arithmetic, block_terms(): lax.linalg.triangular_solve(system, sources, left_side=True, lower=True,...  161 us
    ppermute x2, waiting for transfers between devices, from_partner(): lax.ppermute(array, axis, [(i, i ^ 1 << bit) for i in range(lax.axis_size...  91.7 us
    dot_general x16, matrix products, compose(): joined_state = jnp.matmul(earlier[1], later[0], precision=HIGH) + later[1]  32.8 us
    all_to_all x1, blocking collectives, local(): lax.all_to_all(expert_out, ('sp', 'tp'), split_axis=0, concat_axis=2, til...  32.1 us
    dot_general x1, matrix products, block_terms(): jnp.einsum('bhtk,bhtjk,bhjk->bhtj', unit_key, fade_prev, key_vals, precis...  30.3 us
    dot_general x1, matrix products, block_terms(): jnp.einsum('bhtk,bhtjk,bhjk->bhtj', unit_key, fade_prev, pull_key, precis...  29.1 us
    all_to_all x1, blocking collectives, local(): lax.all_to_all(dispatched, ('sp', 'tp'), split_axis=0, concat_axis=0, til...  28.9 us
  transfers between devices with their start and end apart: 6, of which 6 were waited for; matrix products, arithmetic and copies ran while one was open for 5% of the time, Pallas kernels for 0%

commit v1 on v0

v1 whole, which is shorter than its diff:
```python
import functools

import jax
import jax.numpy as jnp
from jax import lax
from jax.experimental import pallas as pl
from jax.experimental.pallas import tpu as pltpu
from jax.sharding import PartitionSpec as P

HEAD = 64
TOPK = 2
STEP_HEADS = 4

GROUP_EPS = 0.00064
NORM_EPS = 1e-06
UNIT_EPS = 1e-06
NT = (((1,), (1,)), ((), ()))
NN = (((1,), (0,)), ((), ()))
TN = (((0,), (0,)), ((), ()))


def split(x):
    high = x.astype(jnp.bfloat16)
    return high, (x - high.astype(jnp.float32)).astype(jnp.bfloat16)


def dot1(a, b, dims=NN):
    return lax.dot_general(a, b, dims, preferred_element_type=jnp.float32)


def dot3(a, b, dims=NN):
    return dot1(a[0], b[0], dims) + (dot1(a[0], b[1], dims) + dot1(a[1], b[0], dims))


def mixer_kernel(q_ref, k_ref, v_ref, r_ref, l_ref, g_ref, local_ref, carry_ref, pair_ref):
    tokens = q_ref.shape[0]
    heads = q_ref.shape[1] // HEAD
    row = lax.broadcasted_iota(jnp.int32, (tokens, tokens), 0)
    col = lax.broadcasted_iota(jnp.int32, (tokens, tokens), 1)
    strict = row > col
    upto = row >= col
    eye = (row == col).astype(jnp.float32)
    ones = upto.astype(jnp.bfloat16)
    small_eye = (
        lax.broadcasted_iota(jnp.int32, (HEAD, HEAD), 0)
        == lax.broadcasted_iota(jnp.int32, (HEAD, HEAD), 1)
    ).astype(jnp.float32)
    log_decay = -jnp.exp(g_ref[...])
    high, rest = split(log_decay)
    low = log_decay - high.astype(jnp.float32) - rest.astype(jnp.float32)
    cumul = dot1(ones, high) + (dot1(ones, rest) + dot1(ones, low.astype(jnp.bfloat16)))
    before = cumul - log_decay
    middle = cumul[tokens // 2 - 1 : tokens // 2, :]
    last = cumul[tokens - 1 : tokens, :]
    grow = jnp.exp(middle - cumul)
    fade_now = jnp.exp(cumul - middle)
    fade_prev = jnp.exp(before - middle)
    start_now = jnp.exp(cumul)
    start_prev = jnp.exp(before)
    tail = jnp.exp(last - cumul)
    queries = q_ref[...].astype(jnp.float32)
    keys = k_ref[...].astype(jnp.float32)
    removal = r_ref[...].astype(jnp.float32)
    rate = 1.0 / (1.0 + jnp.exp(-l_ref[...].astype(jnp.float32)))
    locals_out, carries_out = [], []
    state = []
    for h in range(heads):
        at = slice(h * HEAD, (h + 1) * HEAD)
        part = removal[:, at]
        unit = part * lax.rsqrt(jnp.sum(part * part, axis=1, keepdims=True) + UNIT_EPS)
        pull = unit * rate[:, at]
        lefts = jnp.concatenate((unit * fade_prev[:, at], queries[:, at] * fade_now[:, at]), axis=0)
        rights = jnp.concatenate((pull * grow[:, at], keys[:, at] * grow[:, at]), axis=0)
        gram = dot3(split(lefts), split(rights), NT)
        mix_pull = jnp.where(strict, gram[:tokens, :tokens], 0.0)
        mix_key = jnp.where(strict, gram[:tokens, tokens:], 0.0)
        read_pull = jnp.where(upto, gram[tokens:, :tokens], 0.0)
        read_key = jnp.where(upto, gram[tokens:, tokens:], 0.0)
        state.append([unit, pull, mix_pull, mix_key, read_pull, read_key])
    inverses = []
    size = 1
    quads = []
    while size < tokens:
        quads.append((row // (2 * size) == col // (2 * size)) & (row // size > col // size))
        size *= 2
    inverses = [eye - jnp.where(quads[0], one[2], 0.0) for one in state]
    for quad in quads[1:]:
        parts = [split(x) for x in inverses]
        inner = [
            dot3(split(jnp.where(quad, one[2], 0.0)), x) for one, x in zip(state, parts)
        ]
        inverses = [
            x - dot3(p, split(y)) for x, p, y in zip(inverses, parts, inner)
        ]
    for h in range(heads):
        at = slice(h * HEAD, (h + 1) * HEAD)
        unit, pull, mix_pull, mix_key, read_pull, read_key = state[h]
        values = v_ref[:, at]
        mix = split(mix_key)
        read = split(read_key)
        both = jnp.concatenate((mix_key, read_key), axis=0)
        both = split(both)
        both = dot1(both[0], values) + dot1(both[1], values)
        sources = jnp.concatenate((both[:tokens], unit * start_prev[:, at]), axis=1)
        solved = split(dot3(split(inverses[h]), split(sources)))
        taken = dot3(split(read_pull), solved)
        locals_out.append(both[tokens:] - taken[:, :HEAD])
        carries_out.append(queries[:, at] * start_now[:, at] - taken[:, HEAD:])
        left = dot3(solved, split(pull * tail[:, at]), TN)
        key_tail = split(keys[:, at] * tail[:, at])
        grown = dot1(values, key_tail[0], TN) + dot1(values, key_tail[1], TN)
        shift = small_eye * (jnp.exp(last[:, at]) - 1.0) - left[HEAD:]
        pair_ref[h] = jnp.concatenate((shift, grown - left[:HEAD]), axis=1).astype(pair_ref.dtype)
    local_ref[...] = jnp.concatenate(locals_out, axis=1)
    carry_ref[...] = jnp.concatenate(carries_out, axis=1).astype(carry_ref.dtype)


def mix_here(queries, keys, values, removal, learn, rates):
    tokens, width = queries.shape
    lanes = STEP_HEADS * HEAD
    block = pl.BlockSpec((tokens, lanes), lambda i: (0, i))
    return pl.pallas_call(
        mixer_kernel,
        grid=(width // lanes,),
        in_specs=[block] * 6,
        out_specs=[block, block, pl.BlockSpec((STEP_HEADS, HEAD, 2 * HEAD), lambda i: (i, 0, 0))],
        out_shape=[
            jax.ShapeDtypeStruct((tokens, width), jnp.float32),
            jax.ShapeDtypeStruct((tokens, width), jnp.bfloat16),
            jax.ShapeDtypeStruct((width // HEAD, HEAD, 2 * HEAD), jnp.bfloat16),
        ],
        compiler_params=pltpu.CompilerParams(vmem_limit_bytes=60 * 2**20),
    )(queries, keys, values, removal, learn, rates)


def chain_kernel(pair_ref, out_ref):
    state = jnp.zeros((HEAD, HEAD), jnp.float32)
    count = pair_ref.shape[0]
    for k in range(count):
        out_ref[k] = state.astype(out_ref.dtype)
        if k < count - 1:
            shift = pair_ref[k, :, :HEAD]
            high, low = split(state)
            moved = dot1(high, shift) + dot1(low, shift)
            state = state + moved + pair_ref[k, :, HEAD:].astype(jnp.float32)


def entering_state(pairs, axis):
    heads = pairs.shape[0]
    devices = lax.axis_size(axis)
    pieces = devices // heads
    if pieces > 1:
        pairs = jnp.repeat(pairs, pieces, axis=0)
    mine = lax.all_to_all(pairs, axis, split_axis=0, concat_axis=0, tiled=True)
    states = pl.pallas_call(
        chain_kernel,
        out_shape=jax.ShapeDtypeStruct((devices, HEAD, HEAD), jnp.bfloat16),
    )(mine)
    if pieces > 1:
        rows = HEAD // pieces
        states = lax.dynamic_slice_in_dim(states, lax.axis_index(axis) % pieces * rows, rows, 1)
    back = lax.all_to_all(states, axis, split_axis=0, concat_axis=0, tiled=True)
    return back.reshape(heads, HEAD, HEAD)


def finish_kernel(local_ref, carry_ref, state_ref, gain_ref, out_ref):
    outs = []
    for h in range(local_ref.shape[1] // HEAD):
        at = slice(h * HEAD, (h + 1) * HEAD)
        mixed = local_ref[:, at] + dot1(carry_ref[:, at], state_ref[h], NT)
        centred = mixed - jnp.mean(mixed, axis=1, keepdims=True)
        variance = jnp.mean(centred * centred, axis=1, keepdims=True)
        outs.append(centred * lax.rsqrt(variance + GROUP_EPS))
    normed = jnp.concatenate(outs, axis=1) * gain_ref[...].astype(jnp.float32)
    out_ref[...] = normed.astype(jnp.bfloat16)


def finish(local_read, carry_read, states, gain):
    return pl.pallas_call(
        finish_kernel, out_shape=jax.ShapeDtypeStruct(local_read.shape, jnp.bfloat16)
    )(local_read, carry_read, states, gain[None, :])


def from_partner(array, axis, bit):
    return lax.ppermute(array, axis, [(i, i ^ 1 << bit) for i in range(lax.axis_size(axis))])


def local(
    stream_in,
    query_rows,
    key_rows,
    value_rows,
    removal_key,
    learn_pre,
    log_rate,
    norm_gain,
    out_weight,
    ffn_gain,
    routes,
    route_weight,
    expert_gate,
    expert_up,
    expert_down,
):
    local_read, carry_read, pairs = mix_here(
        query_rows, key_rows, value_rows, removal_key, learn_pre, log_rate
    )
    states = entering_state(pairs, "sp")
    normed = finish(local_read, carry_read, states, norm_gain)
    gathered = lax.all_to_all(normed, "tp", split_axis=0, concat_axis=1, tiled=True)
    attended = stream_in.astype(jnp.float32) + jnp.dot(
        gathered, out_weight, preferred_element_type=jnp.float32
    )
    scaling = lax.rsqrt(jnp.mean(attended * attended, axis=-1, keepdims=True) + NORM_EPS)
    ffn_in = (attended * scaling * ffn_gain.astype(jnp.float32)).astype(jnp.bfloat16)
    half_rows = attended.shape[0]
    width = attended.shape[1]
    experts = lax.axis_size("sp") // 2
    peers = lax.axis_size("sp") * lax.axis_size("tp")
    capacity = 2 * TOPK * half_rows // experts
    pairs = half_rows * TOPK
    expert_ids = routes.reshape(pairs)
    one_hot = (expert_ids[:, None] == jnp.arange(experts, dtype=jnp.int32)[None, :]).astype(
        jnp.int32
    )
    slot_index = jnp.sum(jnp.cumsum(one_hot, axis=0) * one_hot, axis=1) - 1
    send_index = expert_ids * capacity + slot_index
    send_map = (
        jnp.arange(experts * capacity, dtype=jnp.int32)[:, None] == send_index[None, :]
    ).astype(jnp.bfloat16)
    send_map = jnp.sum(send_map.reshape(experts * capacity, half_rows, TOPK), axis=2)
    dispatched = jnp.dot(send_map, ffn_in, preferred_element_type=jnp.float32).astype(jnp.bfloat16)
    quarters = lax.all_to_all(dispatched, ("sp", "tp"), split_axis=0, concat_axis=0, tiled=True)
    quarters = quarters.reshape(peers, capacity // 4, width)
    partner = from_partner(quarters, "sp", 0)
    even = lax.axis_index("sp") % 2 == 0
    both_chips = jnp.stack((jnp.where(even, quarters, partner), jnp.where(even, partner, quarters)))
    routed = lax.all_gather(both_chips, "tp", axis=2, tiled=True)
    routed = routed.transpose(1, 0, 2, 3).reshape(peers * capacity, width)
    gate_act = jnp.dot(routed, expert_gate[0], preferred_element_type=jnp.float32)
    up_act = jnp.dot(routed, expert_up[0], preferred_element_type=jnp.float32)
    hidden = (jax.nn.silu(gate_act) * up_act).astype(jnp.bfloat16)
    partial_out = jnp.dot(hidden, expert_down[0], preferred_element_type=jnp.float32).astype(
        jnp.bfloat16
    )
    partial_out = partial_out.reshape(peers, capacity, width)
    pair_bit = lax.axis_index("sp") % 2
    core_sum = lax.psum_scatter(partial_out, "tp", scatter_dimension=2, tiled=True)
    part_width = core_sum.shape[2] // 2
    kept = lax.dynamic_slice_in_dim(core_sum, pair_bit * part_width, part_width, 2)
    sent = lax.dynamic_slice_in_dim(core_sum, (1 - pair_bit) * part_width, part_width, 2)
    arrived = from_partner(sent, "sp", 0)
    expert_out = (kept.astype(jnp.float32) + arrived.astype(jnp.float32)).astype(jnp.bfloat16)
    returned = lax.all_to_all(expert_out, ("sp", "tp"), split_axis=0, concat_axis=2, tiled=True)
    returned = returned.reshape(capacity * experts, width)
    back_index = slot_index * experts + expert_ids
    back_map = (
        back_index[:, None] == jnp.arange(capacity * experts, dtype=jnp.int32)[None, :]
    ).astype(jnp.bfloat16)
    picked = jnp.dot(back_map, returned, preferred_element_type=jnp.float32).reshape(
        half_rows, TOPK, width
    )
    mixture = jnp.sum(picked * route_weight[:, :, None], axis=1)
    quarters = jnp.split(mixture, 4, axis=1)
    mixture = jnp.concatenate((quarters[0], quarters[2], quarters[1], quarters[3]), axis=1)
    return (attended + mixture).astype(jnp.bfloat16)


def solution(mesh):
    placed = (
        P(("sp", "tp"), None),
        P("sp", "tp"),
        P("sp", "tp"),
        P("sp", "tp"),
        P("sp", "tp"),
        P("sp", "tp"),
        P("sp", "tp"),
        P("tp"),
        P(),
        P(),
        P(("sp", "tp"), None),
        P(("sp", "tp"), None),
        P("sp", None, "tp"),
        P("sp", None, "tp"),
        P("sp", "tp", None),
    )
    return jax.shard_map(
        local, mesh=mesh, in_specs=placed, out_specs=P(("sp", "tp"), None), check_vma=False
    )
```

time: 868 us -> 250 us (0.29)
  waiting for transfers between devices: 300 us -> 86.9 us
  matrix products: 233 us -> 24.2 us
  other arithmetic: 186 us -> 5.22 us
  local copies, waits for them, and re-layouts: 57.9 us -> 8.48 us
  Pallas kernels: 0 us -> 30.5 us
  starting transfers between devices: 3.63 us -> 15.6 us
    dot_general x45 -> x0, matrix products: 211 us -> none  [the longest x16 32.8 us: compose(): joined_state = jnp.matmul(earlier[1], later[0], precision=HIGH) + later[1]]
    all_gather x3 -> x1, waiting for transfers between devices: 197 us -> 12.9 us  [local(): routed = lax.all_gather(both_chips, 'tp', axis=2, tiled=True)]
    another operation x8 -> x2, other arithmetic: 167 us -> 1.64 us  [local(): jnp.stack((jnp.where(even, quarters, partner), jnp.where(even, partner, q...]
    ppermute x2, waiting for transfers between devices: 91.7 us -> 46.8 us  [from_partner(): lax.ppermute(array, axis, [(i, i ^ 1 << bit) for i in range(lax.axis_size...]
    pallas_call x0 -> x3, Pallas kernels: none -> 30.5 us  [the longest x1 21.7 us: mix_here(): pl.pallas_call(mixer_kernel, grid=(width // lanes,), in_specs=[block] * 6...]
    dynamic_slice x33 -> x1, local copies, waits for them, and re-layouts: 22 us -> 1.3 us  [local(): lax.dynamic_slice_in_dim(core_sum, (1 - pair_bit) * part_width, part_widt...]
    dynamic_update_slice x24 -> x0, local copies, waits for them, and re-layouts: 15.1 us -> none  [local(): lax.scan(across_blocks, (identity, nothing), (block_map, block_state))]
    all_to_all x0 -> x2, waiting for transfers between devices: none -> 13.9 us  [the longest x1 7.63 us: entering_state(): back = lax.all_to_all(states, axis, split_axis=0, concat_axis=0, tiled=True)]
  transfers between devices with their start and end apart: 6 -> 6, of which waited for: 6 -> 6; matrix products, arithmetic and copies ran while one was open for 5% -> 1% of each run, Pallas kernels for 0% -> 0%
where the time goes in v1:
time: 250 us; the launch traced here: 249 us
  waiting for transfers between devices  86.9 us (35%)
  blocking collectives  64.7 us (26%)
  Pallas kernels  30.5 us (12%)
  matrix products  24.2 us (10%)
  starting transfers between devices  15.6 us (6%)
  between operations  13.6 us (5%)
  local copies, waits for them, and re-layouts  8.48 us (3%)
  other arithmetic  5.22 us (2%)
    ppermute x2, waiting for transfers between devices, from_partner(): lax.ppermute(array, axis, [(i, i ^ 1 << bit) for i in range(lax.axis_size...  46.8 us
    all_to_all x1, blocking collectives, local(): lax.all_to_all(expert_out, ('sp', 'tp'), split_axis=0, concat_axis=2, til...  31.7 us
    all_to_all x1, blocking collectives, local(): lax.all_to_all(dispatched, ('sp', 'tp'), split_axis=0, concat_axis=0, til...  27.9 us
    pallas_call x1, Pallas kernels, mix_here(): pl.pallas_call(mixer_kernel, grid=(width // lanes,), in_specs=[block] * 6...  21.7 us
    reduce_scatter x1, waiting for transfers between devices, local(): lax.psum_scatter(partial_out, 'tp', scatter_dimension=2, tiled=True)  13.2 us
    all_gather x1, waiting for transfers between devices, local(): routed = lax.all_gather(both_chips, 'tp', axis=2, tiled=True)  12.9 us
    all_to_all x1, starting transfers between devices, entering_state(): mine = lax.all_to_all(pairs, axis, split_axis=0, concat_axis=0, tiled=True)  8.35 us
    all_to_all x1, waiting for transfers between devices, entering_state(): back = lax.all_to_all(states, axis, split_axis=0, concat_axis=0, tiled=True)  7.63 us
  transfers between devices with their start and end apart: 6, of which 6 were waited for; matrix products, arithmetic and copies ran while one was open for 1% of the time, Pallas kernels for 0%

profile of v1, /device:TPU:0, one launch (start us, length us, event | category | flops | bytes accessed | tf_op | source)
XLA Modules:
  0.0 249.1 jit_solution(7187696159501137381)
XLA Ops:
  6.5 0.0 copy-start.2
  6.5 0.0 copy-start.1
  6.5 21.7 %shard_map.145 = (f32[128,1024]{1,0:T(8,128)}, bf16[128,1024]{1,0:T(8,128)(2,1)}, bf16[16,64,128]{2,1,0:T(8,128)(2,1)}) custom-call(bf16[128,1024]{1,0:T(8,128)(2,1)} %q_ref.1, bf16[128,1024]{1,0:T(8,128)(2,1)} %k_ref.1, bf16[128,1024]{1,0:T(8,128)(2,1)} %v_ref.1, bf16[128,1024]{1,0:T(8,128)(2,1)} %r_ref.1, bf16[128,1024]{1,0:T(8,128)(2,1)} %l_ref.1, ...), custom_call_target="tpu_custom_call" | custom-call | tf_op jit(solution)/shard_map/pallas_call | solution.py:122
  28.3 8.3 %all-to-all-start = ((bf16[16,64,128]{2,1,0:T(8,128)(2,1)}), bf16[16,64,128]{2,1,0:T(8,128)(2,1)S(1)}, u32[]{:S(2)}, u32[]{:S(2)}) async-start(bf16[16,64,128]{2,1,0:T(8,128)(2,1)} %get-tuple-element.10), calls=%async_computation | async-start | bytes 524288 | tf_op jit(solution)/shard_map/all_to_all | solution.py:154
  36.6 1.3 broadcast_in_dim.2.gain_ref
  37.9 0.8 copy.48
  38.7 0.1 eq.64
  38.8 0.1 fusion.17
  38.9 0.2 reduce_window_sum.11
  39.1 0.2 select_reduce_fusion
  39.3 0.1 sub.10
  39.4 0.1 copy.49
  39.5 0.7 convert_element_type.43
  40.2 6.3 %all-to-all-done.pair_ref = bf16[16,64,128]{2,1,0:T(8,128)(2,1)S(1)} async-done(((bf16[16,64,128]{2,1,0:T(8,128)(2,1)}), bf16[16,64,128]{2,1,0:T(8,128)(2,1)S(1)}, u32[]{:S(2)}, u32[]{:S(2)}) %all-to-all-start) | async-done | bytes 262176 | tf_op jit(solution)/shard_map/all_to_all | solution.py:154
  46.5 0.0 copy-start
  46.5 0.7 copy-done
  47.2 3.6 %shard_map.146 = bf16[16,64,64]{2,1,0:T(8,128)(2,1)} custom-call(bf16[16,64,128]{2,1,0:T(8,128)(2,1)} %copy-done), custom_call_target="tpu_custom_call" | custom-call | tf_op jit(solution)/shard_map/pallas_call | solution.py:155
  50.8 1.8 reshape.87
  52.7 3.5 %all-to-all-start.1 = ((bf16[16,2,2048]{2,1,0:T(2,128)(2,1)}), bf16[16,2,2048]{2,1,0:T(2,128)(2,1)S(1)}, u32[]{:S(2)}, u32[]{:S(2)}) async-start(bf16[16,2,2048]{2,1,0:T(2,128)(2,1)} %reshape.87), calls=%async_computation.1 | async-start | bytes 262144 | tf_op jit(solution)/shard_map/all_to_all | solution.py:162
  56.2 0.0 all-gather.2.cloned.1.call-start
  56.3 0.0 copy-done.2
  56.3 0.1 fusion.15
  56.4 7.6 %all-to-all-done.1 = bf16[16,2,2048]{2,1,0:T(2,128)(2,1)S(1)} async-done(((bf16[16,2,2048]{2,1,0:T(2,128)(2,1)}), bf16[16,2,2048]{2,1,0:T(2,128)(2,1)S(1)}, u32[]{:S(2)}, u32[]{:S(2)}) %all-to-all-start.1) | async-done | bytes 131104 | tf_op jit(solution)/shard_map/all_to_all | solution.py:162
  64.0 0.9 reshape.88.state_ref
  64.9 5.1 %shard_map.147 = bf16[128,1024]{1,0:T(8,128)(2,1)} custom-call(f32[128,1024]{1,0:T(8,128)} %get-tuple-element.8.local_ref, bf16[128,1024]{1,0:T(8,128)(2,1)} %get-tuple-element.9.carry_ref, bf16[16,64,64]{2,1,0:T(8,128)(2,1)} %reshape.88.state_ref, bf16[1,1024]{1,0:T(2,128)(2,1)} %broadcast_in_dim.2.gain_ref), custom_call_target="tpu_custom_call" | custom-call | tf_op jit(solution)/shard_map/pallas_call | solution.py:179
  70.0 5.0 %all_to_all.53 = bf16[2,64,1024]{2,1,0:T(8,128)(2,1)S(1)} all-to-all(bf16[2,64,1024]{2,1,0:T(8,128)(2,1)} %bitcast.45), channel_id=1, replica_groups=mesh['sp'=16,'tp'=2] {'tp'}, dimensions={0} | all-to-all | bytes 524288 | tf_op jit(solution)/shard_map/all_to_all | solution.py:210
  75.1 0.0 copy-done.1
  75.1 5.1 %multiply_reduce_fusion = (f32[64]{0:T(128)S(1)}, f32[64,2048]{1,0:T(8,128)S(1)}) fusion(bf16[64,2048]{1,0:T(8,128)(2,1)S(1)} %bitcast.44, bf16[2048,2048]{1,0:T(8,128)(2,1)} %param.23, bf16[64,2048]{1,0:T(8,128)(2,1)S(1)} %copy-done.1), kind=kOutput, calls=%fused_computation.19 | convolution fusion | flops 537395136 | bytes 9437440 | tf_op jit(solution)/shard_map/dot_general | solution.py:211
  80.2 0.5 fusion.7
  80.7 27.9 %all_to_all.54 = bf16[32,8,2048]{2,1,0:T(8,128)(2,1)S(1)} all-to-all(bf16[32,8,2048]{2,1,0:T(8,128)(2,1)S(1)} %fusion.7), channel_id=1, replica_groups=mesh['sp'=16,'tp'=2] {'sp','tp'}, dimensions={0} | all-to-all | bytes 2097152 | tf_op jit(solution)/shard_map/all_to_all | solution.py:233
  108.6 1.5 collective-permute-start
  110.1 23.2 %collective-permute-done = bf16[32,8,2048]{2,1,0:T(8,128)(2,1)S(1)} collective-permute-done((bf16[32,8,2048]{2,1,0:T(8,128)(2,1)S(1)}, bf16[32,8,2048]{2,1,0:T(8,128)(2,1)S(1)}, u32[]{:S(2)}, u32[]{:S(2)}) %collective-permute-start) | collective-permute-done | bytes 1048608 | tf_op jit(solution)/shard_map/ppermute | solution.py:185
  133.3 0.1 select_bitcast_fusion.1
  133.5 1.5 pad_maximum_fusion
  135.0 0.0 all-gather.2.cloned.1.call-update
  135.0 0.2 reduce-scatter.2.cloned.1.call-start
  135.2 12.9 %all-gather.2.cloned.1.call-done = bf16[2,32,16,2048]{3,2,0,1:T(8,128)(2,1)} async-done(((bf16[2,32,8,2048]{3,2,0,1:T(8,128)(2,1)}), bf16[2,32,16,2048]{3,2,0,1:T(8,128)(2,1)}) %all-gather.2.cloned.1.call-update) | async-done | bytes 4194320 | tf_op jit(solution)/shard_map/all_gather | solution.py:238
  148.2 0.0 copy-start.4
  148.2 0.0 copy-start.5
  148.2 7.5 %fusion.1 = f32[1024,896]{1,0:T(8,128)S(1)} fusion(bf16[1024,2048]{1,0:T(8,128)(2,1)} %bitcast.47, bf16[1,2048,896]{2,1,0:T(8,128)(2,1)} %param.28), kind=kOutput, calls=%fused_computation.2 | convolution fusion | flops 3758096384 | bytes 11534336 | tf_op jit(solution)/shard_map/dot_general | solution.py:241
  155.7 0.0 copy-done.4
  155.7 0.0 copy-done.5
  155.7 0.0 copy-start.6
  155.7 4.7 %multiply_convert_fusion = bf16[1024,896]{1,0:T(8,128)(2,1)S(1)} fusion(f32[1024,896]{1,0:T(8,128)S(1)} %fusion.1, bf16[1024,2048]{1,0:T(8,128)(2,1)S(1)} %bitcast.48, bf16[1,2048,896]{2,1,0:T(8,128)(2,1)S(1)} %copy-done.5), kind=kOutput, calls=%fused_computation.6 | convolution fusion | flops 3763601408 | bytes 13369344 | tf_op jit(solution)/shard_map/dot_general | solution.py:240
  160.5 0.0 copy-done.6
  160.5 6.0 %convolution_convert_fusion = bf16[1024,2048]{1,0:T(8,128)(2,1)} fusion(bf16[1024,896]{1,0:T(8,128)(2,1)S(1)} %multiply_convert_fusion, bf16[1,896,2048]{2,1,0:T(8,128)(2,1)S(1)} %copy-done.6), kind=kOutput, calls=%fused_computation | convolution fusion | flops 3760193536 | bytes 9699328 | tf_op jit(solution)/shard_map/dot_general | solution.py:243
  166.5 0.0 reduce-scatter.2.cloned.1.call-update
  166.5 13.2 %reduce-scatter.2.cloned.1.call-done = bf16[32,32,1024]{2,1,0:T(8,128)(2,1)} async-done(((bf16[32,32,2048]{2,1,0:T(8,128)(2,1)}), bf16[32,32,1024]{2,1,0:T(8,128)(2,1)}) %reduce-scatter.2.cloned.1.call-update) | async-done | bytes 2097168 | tf_op jit(solution)/shard_map/reduce_scatter | solution.py:248
  179.7 1.3 constant_dynamic-slice_fusion
  181.0 1.9 collective-permute-start.1
  183.0 23.5 %collective-permute-done.1 = bf16[32,32,512]{2,1,0:T(8,128)(2,1)S(1)} collective-permute-done((bf16[32,32,512]{2,1,0:T(8,128)(2,1)S(1)}, bf16[32,32,512]{2,1,0:T(8,128)(2,1)S(1)}, u32[]{:S(2)}, u32[]{:S(2)}) %collective-permute-start.1) | collective-permute-done | bytes 1048608 | tf_op jit(solution)/shard_map/ppermute | solution.py:185
  206.5 1.6 add_convert_fusion
  208.1 0.0 copy-start.3
  208.1 31.7 %all_to_all.55 = bf16[32,32,512]{2,1,0:T(8,128)(2,1)S(1)} all-to-all(bf16[32,32,512]{2,1,0:T(8,128)(2,1)S(1)} %add_convert_fusion), channel_id=1, replica_groups=mesh['sp'=16,'tp'=2] {'sp','tp'}, dimensions={0} | all-to-all | bytes 2097152 | tf_op jit(solution)/shard_map/all_to_all | solution.py:254
  239.9 0.6 copy.52
  240.4 0.7 reshape.85
  241.1 0.0 copy-done.3
  241.1 0.4 fusion.8
  241.5 0.8 fusion.9
  (5 shorter events, 0.1 us)
Async XLA Ops:
  6.5 49.8 %copy-start.2 = (s32[64,2]{0,1:T(2,128)S(1)}, s32[64,2]{0,1:T(2,128)}, u32[]{:S(2)}) copy-start(s32[64,2]{0,1:T(2,128)} %param.25) | copy-start | bytes 1540
  6.5 68.5 %copy-start.1 = (bf16[64,2048]{1,0:T(8,128)(2,1)S(1)}, bf16[64,2048]{1,0:T(8,128)(2,1)}, u32[]{:S(2)}) copy-start(bf16[64,2048]{1,0:T(8,128)(2,1)} %param.15) | copy-start | bytes 786436
  28.3 18.2 %all-to-all-start = ((bf16[16,64,128]{2,1,0:T(8,128)(2,1)}), bf16[16,64,128]{2,1,0:T(8,128)(2,1)S(1)}, u32[]{:S(2)}, u32[]{:S(2)}) async-start(bf16[16,64,128]{2,1,0:T(8,128)(2,1)} %get-tuple-element.10), calls=%async_computation | async-start | bytes 524288 | tf_op jit(solution)/shard_map/all_to_all | solution.py:154
  46.5 0.7 copy-start
  52.7 11.3 %all-to-all-start.1 = ((bf16[16,2,2048]{2,1,0:T(2,128)(2,1)}), bf16[16,2,2048]{2,1,0:T(2,128)(2,1)S(1)}, u32[]{:S(2)}, u32[]{:S(2)}) async-start(bf16[16,2,2048]{2,1,0:T(2,128)(2,1)} %reshape.87), calls=%async_computation.1 | async-start | bytes 262144 | tf_op jit(solution)/shard_map/all_to_all | solution.py:162
  56.2 91.9 %all-gather.2.cloned.1.call-start = ((), (), s32[]{:S(2)}) async-start(), calls=%async_computation.6 | async-start | bytes 6291456 | tf_op jit(solution)/shard_map/all_gather | solution.py:238
  108.6 24.7 %collective-permute-start = (bf16[32,8,2048]{2,1,0:T(8,128)(2,1)S(1)}, bf16[32,8,2048]{2,1,0:T(8,128)(2,1)S(1)}, u32[]{:S(2)}, u32[]{:S(2)}) collective-permute-start(bf16[32,8,2048]{2,1,0:T(8,128)(2,1)S(1)} %all_to_all.54), channel_id=1, source_target_pairs={{0,2},{2,0},{4,6},{6,4},{8,10},{10,8},{12,14},{14,12},{16,18},{18,... | collective-permute-start | bytes 3145736 | tf_op jit(solution)/shard_map/ppermute | solution.py:185
  135.0 44.7 %reduce-scatter.2.cloned.1.call-start = ((), (), s32[]{:S(2)}) async-start(), calls=%async_computation.7 | async-start | bytes 6291456 | tf_op jit(solution)/shard_map/reduce_scatter | solution.py:248
  148.2 7.5 %copy-start.4 = (bf16[2,32,16,2048]{3,2,0,1:T(8,128)(2,1)S(1)}, bf16[2,32,16,2048]{3,2,0,1:T(8,128)(2,1)}, u32[]{:S(2)}) copy-start(bf16[2,32,16,2048]{3,2,0,1:T(8,128)(2,1)} %all-gather.2.cloned.1.call-done) | copy-start | bytes 12582916
  148.2 7.5 %copy-start.5 = (bf16[1,2048,896]{2,1,0:T(8,128)(2,1)S(1)}, bf16[1,2048,896]{2,1,0:T(8,128)(2,1)}, u32[]{:S(2)}) copy-start(bf16[1,2048,896]{2,1,0:T(8,128)(2,1)} %param.27) | copy-start | bytes 11010052
  155.7 4.8 %copy-start.6 = (bf16[1,896,2048]{2,1,0:T(8,128)(2,1)S(1)}, bf16[1,896,2048]{2,1,0:T(8,128)(2,1)}, u32[]{:S(2)}) copy-start(bf16[1,896,2048]{2,1,0:T(8,128)(2,1)} %param.29) | copy-start | bytes 11010052
  181.0 25.5 %collective-permute-start.1 = (bf16[32,32,512]{2,1,0:T(8,128)(2,1)S(1)}, bf16[32,32,512]{2,1,0:T(8,128)(2,1)S(1)}, u32[]{:S(2)}, u32[]{:S(2)}) collective-permute-start(bf16[32,32,512]{2,1,0:T(8,128)(2,1)S(1)} %constant_dynamic-slice_fusion), channel_id=1, source_target_pairs={{0,2},{2,0},{4,6},{6,4},{8,10},{10,8},{12,14},{14,12},{16,18},{18,... | collective-permute-start | bytes 3145736 | tf_op jit(solution)/shard_map/ppermute | solution.py:185
  208.1 33.0 %copy-start.3 = (f32[64,2]{0,1:T(2,128)S(1)}, f32[64,2]{0,1:T(2,128)}, u32[]{:S(2)}) copy-start(f32[64,2]{0,1:T(2,128)} %param.26) | copy-start | bytes 1540
Sparse Core Ops, SparseCore 0:
  135.1 13.0 all-gather.1
  166.7 13.0 reduce-scatter.1

commit v2 on v1

--- a/solution.py
+++ b/solution.py
@@ -181,8 +181,178 @@
     )(local_read, carry_read, states, gain[None, :])
 
 
-def from_partner(array, axis, bit):
-    return lax.ppermute(array, axis, [(i, i ^ 1 << bit) for i in range(lax.axis_size(axis))])
+MESH = pl.DeviceIdType.MESH
+
+
+def places():
+    sp, core = lax.axis_index("sp"), lax.axis_index("tp")
+    group, side = sp // 2, sp % 2
+    return sp, core, group, side
+
+
+def greet(groups, sp, core, group, side):
+    barrier = pltpu.get_barrier_semaphore()
+    others = [((group + o) % groups * 2 + side, core) for o in range(1, groups)]
+    others += [(group * 2 + 1 - side, core), (sp, 1 - core)]
+    for other in others:
+        pl.semaphore_signal(barrier, inc=1, device_id=other, device_id_type=MESH)
+    pl.semaphore_wait(barrier, len(others))
+
+
+def remote(source, target, send, recv, device):
+    return pltpu.make_async_remote_copy(
+        src_ref=source,
+        dst_ref=target,
+        send_sem=send,
+        recv_sem=recv,
+        device_id=device,
+        device_id_type=MESH,
+    )
+
+
+def dispatch_kernel(rows_ref, out_ref, own_sem, send_sem, recv_sem):
+    groups = rows_ref.shape[0]
+    sp, core, group, side = places()
+    across, beside = (group * 2 + 1 - side, core), (sp, 1 - core)
+    greet(groups, sp, core, group, side)
+    own = pltpu.make_async_copy(rows_ref.at[group], out_ref.at[group, side, core], own_sem)
+    own.start()
+    first = {}
+    for o in range(1, groups):
+        to = (group + o) % groups
+        first[o] = remote(
+            rows_ref.at[to],
+            out_ref.at[group, side, core],
+            send_sem.at[0, o],
+            recv_sem.at[0, o],
+            (to * 2 + side, core),
+        )
+        first[o].start()
+    over, near, last = {}, {}, {}
+    lag = 2
+    for o in range(groups + lag):
+        if o < groups:
+            source = (group + groups - o) % groups
+            if o == 0:
+                own.wait()
+            else:
+                first[o].wait_recv()
+            block = out_ref.at[source, side, core]
+            over[o] = remote(block, block, send_sem.at[1, o], recv_sem.at[1, o], across)
+            near[o] = remote(block, block, send_sem.at[2, o], recv_sem.at[2, o], beside)
+            over[o].start()
+            near[o].start()
+        if o >= lag:
+            p = o - lag
+            source = (group + groups - p) % groups
+            over[p].wait_recv()
+            block = out_ref.at[source, 1 - side, core]
+            last[p] = remote(block, block, send_sem.at[3, p], recv_sem.at[3, p], beside)
+            last[p].start()
+    for o in range(groups):
+        near[o].wait_recv()
+        last[o].wait_recv()
+        if o > 0:
+            first[o].wait_send()
+        over[o].wait_send()
+        near[o].wait_send()
+        last[o].wait_send()
+
+
+def dispatch(rows):
+    groups, capacity, width = rows.shape
+    return pl.pallas_call(
+        dispatch_kernel,
+        out_shape=jax.ShapeDtypeStruct((groups, 2, 2, capacity, width), rows.dtype),
+        in_specs=[pl.BlockSpec(memory_space=pltpu.VMEM)],
+        out_specs=pl.BlockSpec(memory_space=pltpu.VMEM),
+        scratch_shapes=[
+            pltpu.SemaphoreType.DMA,
+            pltpu.SemaphoreType.DMA((4, groups)),
+            pltpu.SemaphoreType.DMA((4, groups)),
+        ],
+        compiler_params=pltpu.CompilerParams(
+            collective_id=0, has_side_effects=True, vmem_limit_bytes=40 * 2**20
+        ),
+    )(rows)
+
+
+def add(a, b):
+    return a.astype(jnp.float32) + b.astype(jnp.float32)
+
+
+def give_back_kernel(part_ref, out_ref, core_in, core_sum, side_in, total, send_sem, recv_sem):
+    groups = part_ref.shape[0]
+    sp, core, group, side = places()
+    across, beside = (group * 2 + 1 - side, core), (sp, 1 - core)
+    greet(groups, sp, core, group, side)
+    order = list(range(1, groups)) + [0]
+    cores, sides, finals = {}, {}, {}
+    for kind, which in ((0, 1 - side), (1, side)):
+        for o in order:
+            to = (group + o) % groups
+            cores[kind, o] = remote(
+                part_ref.at[to, which, 1 - core],
+                core_in.at[to, which],
+                send_sem.at[kind, o],
+                recv_sem.at[kind, o],
+                beside,
+            )
+            cores[kind, o].start()
+    for o in order:
+        to = (group + o) % groups
+        cores[0, o].wait_recv()
+        core_sum[to] = add(part_ref[to, 1 - side, core], core_in[to, 1 - side]).astype(core_sum.dtype)
+        sides[o] = remote(
+            core_sum.at[to], side_in.at[to], send_sem.at[2, o], recv_sem.at[2, o], across
+        )
+        sides[o].start()
+    for o in order:
+        to = (group + o) % groups
+        cores[1, o].wait_recv()
+        sides[o].wait_recv()
+        kept = add(part_ref[to, side, core], core_in[to, side])
+        summed = (kept + side_in[to].astype(jnp.float32)).astype(total.dtype)
+        if o == 0:
+            out_ref[to] = summed
+        else:
+            total[to] = summed
+            finals[o] = remote(
+                total.at[to],
+                out_ref.at[group],
+                send_sem.at[3, o],
+                recv_sem.at[3, o],
+                (to * 2 + side, core),
+            )
+            finals[o].start()
+    for o in order:
+        if o > 0:
+            finals[o].wait()
+        sides[o].wait_send()
+        cores[0, o].wait_send()
+        cores[1, o].wait_send()
+
+
+def give_back(parts):
+    groups, _, _, capacity, width = parts.shape
+    block = (groups, capacity, width)
+    return pl.pallas_call(
+        give_back_kernel,
+        out_shape=jax.ShapeDtypeStruct(block, parts.dtype),
+        in_specs=[pl.BlockSpec(memory_space=pltpu.VMEM)],
+        out_specs=pl.BlockSpec(memory_space=pltpu.VMEM),
+        scratch_shapes=[
+            pltpu.VMEM((groups, 2, capacity, width), parts.dtype),
+            pltpu.VMEM(block, parts.dtype),
+            pltpu.VMEM(block, parts.dtype),
+            pltpu.VMEM(block, parts.dtype),
+            pltpu.SemaphoreType.DMA((4, groups)),
+            pltpu.SemaphoreType.DMA((4, groups)),
+        ],
+        compiler_params=pltpu.CompilerParams(
+            collective_id=1, has_side_effects=True, vmem_limit_bytes=40 * 2**20
+        ),
+    )(parts)
 
 
 def local(
@@ -230,39 +400,22 @@
     ).astype(jnp.bfloat16)
     send_map = jnp.sum(send_map.reshape(experts * capacity, half_rows, TOPK), axis=2)
     dispatched = jnp.dot(send_map, ffn_in, preferred_element_type=jnp.float32).astype(jnp.bfloat16)
-    quarters = lax.all_to_all(dispatched, ("sp", "tp"), split_axis=0, concat_axis=0, tiled=True)
-    quarters = quarters.reshape(peers, capacity // 4, width)
-    partner = from_partner(quarters, "sp", 0)
-    even = lax.axis_index("sp") % 2 == 0
-    both_chips = jnp.stack((jnp.where(even, quarters, partner), jnp.where(even, partner, quarters)))
-    routed = lax.all_gather(both_chips, "tp", axis=2, tiled=True)
-    routed = routed.transpose(1, 0, 2, 3).reshape(peers * capacity, width)
+    arrived = dispatch(dispatched.reshape(experts, capacity, width))
+    routed = arrived.reshape(peers * capacity, width)
     gate_act = jnp.dot(routed, expert_gate[0], preferred_element_type=jnp.float32)
     up_act = jnp.dot(routed, expert_up[0], preferred_element_type=jnp.float32)
     hidden = (jax.nn.silu(gate_act) * up_act).astype(jnp.bfloat16)
     partial_out = jnp.dot(hidden, expert_down[0], preferred_element_type=jnp.float32).astype(
         jnp.bfloat16
     )
-    partial_out = partial_out.reshape(peers, capacity, width)
-    pair_bit = lax.axis_index("sp") % 2
-    core_sum = lax.psum_scatter(partial_out, "tp", scatter_dimension=2, tiled=True)
-    part_width = core_sum.shape[2] // 2
-    kept = lax.dynamic_slice_in_dim(core_sum, pair_bit * part_width, part_width, 2)
-    sent = lax.dynamic_slice_in_dim(core_sum, (1 - pair_bit) * part_width, part_width, 2)
-    arrived = from_partner(sent, "sp", 0)
-    expert_out = (kept.astype(jnp.float32) + arrived.astype(jnp.float32)).astype(jnp.bfloat16)
-    returned = lax.all_to_all(expert_out, ("sp", "tp"), split_axis=0, concat_axis=2, tiled=True)
-    returned = returned.reshape(capacity * experts, width)
-    back_index = slot_index * experts + expert_ids
+    returned = give_back(partial_out.reshape(arrived.shape)).reshape(experts * capacity, width)
     back_map = (
-        back_index[:, None] == jnp.arange(capacity * experts, dtype=jnp.int32)[None, :]
+        send_index[:, None] == jnp.arange(experts * capacity, dtype=jnp.int32)[None, :]
     ).astype(jnp.bfloat16)
     picked = jnp.dot(back_map, returned, preferred_element_type=jnp.float32).reshape(
         half_rows, TOPK, width
     )
     mixture = jnp.sum(picked * route_weight[:, :, None], axis=1)
-    quarters = jnp.split(mixture, 4, axis=1)
-    mixture = jnp.concatenate((quarters[0], quarters[2], quarters[1], quarters[3]), axis=1)
     return (attended + mixture).astype(jnp.bfloat16)
 
 

time: 250 us -> 164 us (0.66)
  Pallas kernels: 30.5 us -> 104 us
  waiting for transfers between devices: 86.9 us -> 14 us
  blocking collectives: 64.7 us -> 4.98 us
  between operations: 13.6 us -> 0.21 us
  matrix products: 24.2 us -> 19.9 us
  starting transfers between devices: 15.6 us -> 11.9 us
  other arithmetic: 5.22 us -> 1.97 us
  local copies, waits for them, and re-layouts: 8.48 us -> 5.91 us
    pallas_call x0 -> x2, Pallas kernels: none -> 73.9 us  [the longest x1 38.1 us: give_back(): pl.pallas_call(give_back_kernel, out_shape=jax.ShapeDtypeStruct(block, pa...]
    all_to_all x2 -> x0, blocking collectives: 59.7 us -> none  [the longest x1 31.7 us: local(): lax.all_to_all(expert_out, ('sp', 'tp'), split_axis=0, concat_axis=2, til...]
    ppermute x2 -> x0, waiting for transfers between devices: 46.8 us -> none  [from_partner(): lax.ppermute(array, axis, [(i, i ^ 1 << bit) for i in range(lax.axis_size...]
    reduce_scatter x1 -> x0, waiting for transfers between devices: 13.2 us -> none  [local(): lax.psum_scatter(partial_out, 'tp', scatter_dimension=2, tiled=True)]
    all_gather x1 -> x0, waiting for transfers between devices: 12.9 us -> none  [local(): routed = lax.all_gather(both_chips, 'tp', axis=2, tiled=True)]
    ppermute x2 -> x0, starting transfers between devices: 3.4 us -> none  [from_partner(): lax.ppermute(array, axis, [(i, i ^ 1 << bit) for i in range(lax.axis_size...]
    dot_general x1, matrix products: 7.49 us -> 4.48 us  [local(): up_act = jnp.dot(routed, expert_up[0], preferred_element_type=jnp.float32)]
  transfers between devices with their start and end apart: 6 -> 2, of which waited for: 6 -> 2; matrix products, arithmetic and copies ran while one was open for 1% -> 2% of each run, Pallas kernels for 0% -> 0%
where the time goes in v2:
time: 164 us; the launch traced here: 163 us
  Pallas kernels  104 us (63%)
  matrix products  19.9 us (12%)
  waiting for transfers between devices  14 us (9%)
  starting transfers between devices  11.9 us (7%)
  local copies, waits for them, and re-layouts  5.91 us (4%)
  blocking collectives  4.98 us (3%)
  other arithmetic  1.97 us (1%)
    pallas_call x1, Pallas kernels, give_back(): pl.pallas_call(give_back_kernel, out_shape=jax.ShapeDtypeStruct(block, pa...  38.1 us
    pallas_call x1, Pallas kernels, dispatch(): pl.pallas_call(dispatch_kernel, out_shape=jax.ShapeDtypeStruct((groups, 2...  35.8 us
    pallas_call x1, Pallas kernels, mix_here(): pl.pallas_call(mixer_kernel, grid=(width // lanes,), in_specs=[block] * 6...  21.7 us
    all_to_all x1, starting transfers between devices, entering_state(): mine = lax.all_to_all(pairs, axis, split_axis=0, concat_axis=0, tiled=True)  8.34 us
    all_to_all x1, waiting for transfers between devices, entering_state(): back = lax.all_to_all(states, axis, split_axis=0, concat_axis=0, tiled=True)  7.68 us
    all_to_all x1, waiting for transfers between devices, entering_state(): mine = lax.all_to_all(pairs, axis, split_axis=0, concat_axis=0, tiled=True)  6.33 us
    pallas_call x1, Pallas kernels, finish(): pl.pallas_call(finish_kernel, out_shape=jax.ShapeDtypeStruct(local_read.s...  5.11 us
    dot_general x1, matrix products, local(): jnp.dot(gathered, out_weight, preferred_element_type=jnp.float32)  5.08 us
  transfers between devices with their start and end apart: 2, of which 2 were waited for; matrix products, arithmetic and copies ran while one was open for 2% of the time, Pallas kernels for 0%

profile of v2, /device:TPU:0, one launch (start us, length us, event | category | flops | bytes accessed | tf_op | source)
XLA Modules:
  0.0 163.2 jit_solution(4923914475469834026)
XLA Ops:
  0.0 0.0 copy-start.2
  0.0 0.0 copy-start.1
  0.0 21.7 %shard_map.145 = (f32[128,1024]{1,0:T(8,128)}, bf16[128,1024]{1,0:T(8,128)(2,1)}, bf16[16,64,128]{2,1,0:T(8,128)(2,1)}) custom-call(bf16[128,1024]{1,0:T(8,128)(2,1)} %q_ref.1, bf16[128,1024]{1,0:T(8,128)(2,1)} %k_ref.1, bf16[128,1024]{1,0:T(8,128)(2,1)} %v_ref.1, bf16[128,1024]{1,0:T(8,128)(2,1)} %r_ref.1, bf16[128,1024]{1,0:T(8,128)(2,1)} %l_ref.1, ...), custom_call_target="tpu_custom_call" | custom-call | tf_op jit(solution)/shard_map/pallas_call | solution.py:122
  21.7 8.3 %all-to-all-start = ((bf16[16,64,128]{2,1,0:T(8,128)(2,1)}), bf16[16,64,128]{2,1,0:T(8,128)(2,1)S(1)}, u32[]{:S(2)}, u32[]{:S(2)}) async-start(bf16[16,64,128]{2,1,0:T(8,128)(2,1)} %get-tuple-element.10), calls=%async_computation | async-start | bytes 524288 | tf_op jit(solution)/shard_map/all_to_all | solution.py:154
  30.1 1.3 broadcast_in_dim.2.gain_ref
  31.3 0.7 convert_element_type.34
  32.0 0.8 copy.37
  32.8 0.1 eq.58
  32.9 0.1 fusion.15
  33.0 0.2 reduce_window_sum.11
  33.2 0.2 select_reduce_fusion
  33.4 0.1 sub.7
  33.5 0.1 copy.38
  33.6 6.3 %all-to-all-done.pair_ref = bf16[16,64,128]{2,1,0:T(8,128)(2,1)S(1)} async-done(((bf16[16,64,128]{2,1,0:T(8,128)(2,1)}), bf16[16,64,128]{2,1,0:T(8,128)(2,1)S(1)}, u32[]{:S(2)}, u32[]{:S(2)}) %all-to-all-start) | async-done | bytes 262176 | tf_op jit(solution)/shard_map/all_to_all | solution.py:154
  39.9 0.0 copy-start
  39.9 0.7 copy-done
  40.6 3.6 %shard_map.146 = bf16[16,64,64]{2,1,0:T(8,128)(2,1)} custom-call(bf16[16,64,128]{2,1,0:T(8,128)(2,1)} %copy-done), custom_call_target="tpu_custom_call" | custom-call | tf_op jit(solution)/shard_map/pallas_call | solution.py:155
  44.3 1.8 %reshape.85 = bf16[16,2,2048]{2,1,0:T(2,128)(2,1)} reshape(bf16[16,64,64]{2,1,0:T(8,128)(2,1)} %shard_map.146) | data formatting | bytes 262144
  46.1 3.5 %all-to-all-start.1 = ((bf16[16,2,2048]{2,1,0:T(2,128)(2,1)}), bf16[16,2,2048]{2,1,0:T(2,128)(2,1)S(1)}, u32[]{:S(2)}, u32[]{:S(2)}) async-start(bf16[16,2,2048]{2,1,0:T(2,128)(2,1)} %reshape.85), calls=%async_computation.1 | async-start | bytes 262144 | tf_op jit(solution)/shard_map/all_to_all | solution.py:162
  49.7 0.0 copy-done.2
  49.7 0.1 fusion.13
  49.8 7.7 %all-to-all-done.1 = bf16[16,2,2048]{2,1,0:T(2,128)(2,1)S(1)} async-done(((bf16[16,2,2048]{2,1,0:T(2,128)(2,1)}), bf16[16,2,2048]{2,1,0:T(2,128)(2,1)S(1)}, u32[]{:S(2)}, u32[]{:S(2)}) %all-to-all-start.1) | async-done | bytes 131104 | tf_op jit(solution)/shard_map/all_to_all | solution.py:162
  57.5 0.9 reshape.86.state_ref
  58.4 5.1 %shard_map.147 = bf16[128,1024]{1,0:T(8,128)(2,1)} custom-call(f32[128,1024]{1,0:T(8,128)} %get-tuple-element.8.local_ref, bf16[128,1024]{1,0:T(8,128)(2,1)} %get-tuple-element.9.carry_ref, bf16[16,64,64]{2,1,0:T(8,128)(2,1)} %reshape.86.state_ref, bf16[1,1024]{1,0:T(2,128)(2,1)} %broadcast_in_dim.2.gain_ref), custom_call_target="tpu_custom_call" | custom-call | tf_op jit(solution)/shard_map/pallas_call | solution.py:179
  63.5 5.0 %all_to_all.29 = bf16[2,64,1024]{2,1,0:T(8,128)(2,1)S(1)} all-to-all(bf16[2,64,1024]{2,1,0:T(8,128)(2,1)} %bitcast.37), channel_id=1, replica_groups=mesh['sp'=16,'tp'=2] {'tp'}, dimensions={0} | all-to-all | bytes 524288 | tf_op jit(solution)/shard_map/all_to_all | solution.py:380
  68.5 0.0 copy-done.1
  68.5 5.1 %multiply_reduce_fusion = (f32[64]{0:T(128)S(1)}, f32[64,2048]{1,0:T(8,128)S(1)}) fusion(bf16[64,2048]{1,0:T(8,128)(2,1)S(1)} %bitcast.36, bf16[2048,2048]{1,0:T(8,128)(2,1)} %param.23, bf16[64,2048]{1,0:T(8,128)(2,1)S(1)} %copy-done.1), kind=kOutput, calls=%fused_computation.13 | convolution fusion | flops 537395136 | bytes 9437440 | tf_op jit(solution)/shard_map/dot_general | solution.py:381
  73.6 0.0 copy-start.4
  73.6 0.5 convolution_convert_fusion.1
  74.1 35.8 %shard_map.148 = bf16[8,2,2,32,2048]{4,3,2,1,0:T(8,128)(2,1)S(1)} custom-call(bf16[8,32,2048]{2,1,0:T(8,128)(2,1)S(1)} %bitcast.34), custom_call_target="tpu_custom_call" | custom-call | tf_op jit(solution)/shard_map/pallas_call | solution.py:264
  109.9 0.0 copy-done.4
  109.9 0.0 copy-start.5
  109.9 4.5 %fusion.1 = f32[1024,896]{1,0:T(8,128)S(1)} fusion(bf16[1024,2048]{1,0:T(8,128)(2,1)S(1)} %bitcast.31, bf16[1,2048,896]{2,1,0:T(8,128)(2,1)S(1)} %copy-done.4), kind=kOutput, calls=%fused_computation.2 | convolution fusion | flops 3758096384 | bytes 11534336 | tf_op jit(solution)/shard_map/dot_general | solution.py:406
  114.4 0.0 copy-done.5
  114.4 0.0 copy-start.6
  114.5 4.8 %multiply_convert_fusion = bf16[1024,896]{1,0:T(8,128)(2,1)S(1)} fusion(f32[1024,896]{1,0:T(8,128)S(1)} %fusion.1, bf16[1024,2048]{1,0:T(8,128)(2,1)S(1)} %bitcast.32, bf16[1,2048,896]{2,1,0:T(8,128)(2,1)S(1)} %copy-done.5), kind=kOutput, calls=%fused_computation.6 | convolution fusion | flops 3763601408 | bytes 13369344 | tf_op jit(solution)/shard_map/dot_general | solution.py:405
  119.2 0.0 copy-done.6
  119.2 4.7 %convolution_convert_fusion = bf16[1024,2048]{1,0:T(8,128)(2,1)S(1)} fusion(bf16[1024,896]{1,0:T(8,128)(2,1)S(1)} %multiply_convert_fusion, bf16[1,896,2048]{2,1,0:T(8,128)(2,1)S(1)} %copy-done.6), kind=kOutput, calls=%fused_computation | convolution fusion | flops 3760193536 | bytes 9699328 | tf_op jit(solution)/shard_map/dot_general | solution.py:408
  123.9 0.0 copy-start.3
  124.0 38.1 %shard_map.149 = bf16[8,32,2048]{2,1,0:T(8,128)(2,1)S(1)} custom-call(bf16[8,2,2,32,2048]{4,3,2,1,0:T(8,128)(2,1)S(1)} %bitcast.33), custom_call_target="tpu_custom_call" | custom-call | tf_op jit(solution)/shard_map/pallas_call | solution.py:339
  162.1 0.0 copy-done.3
  162.1 0.4 fusion.7
  162.5 0.8 add_convert_fusion
  (4 shorter events, 0.0 us)
Async XLA Ops:
  0.0 49.7 %copy-start.2 = (s32[64,2]{0,1:T(2,128)S(1)}, s32[64,2]{0,1:T(2,128)}, u32[]{:S(2)}) copy-start(s32[64,2]{0,1:T(2,128)} %param.25) | copy-start | bytes 1540
  0.0 68.5 %copy-start.1 = (bf16[64,2048]{1,0:T(8,128)(2,1)S(1)}, bf16[64,2048]{1,0:T(8,128)(2,1)}, u32[]{:S(2)}) copy-start(bf16[64,2048]{1,0:T(8,128)(2,1)} %param.15) | copy-start | bytes 786436
  21.7 18.2 %all-to-all-start = ((bf16[16,64,128]{2,1,0:T(8,128)(2,1)}), bf16[16,64,128]{2,1,0:T(8,128)(2,1)S(1)}, u32[]{:S(2)}, u32[]{:S(2)}) async-start(bf16[16,64,128]{2,1,0:T(8,128)(2,1)} %get-tuple-element.10), calls=%async_computation | async-start | bytes 524288 | tf_op jit(solution)/shard_map/all_to_all | solution.py:154
  39.9 0.7 copy-start
  46.1 11.3 %all-to-all-start.1 = ((bf16[16,2,2048]{2,1,0:T(2,128)(2,1)}), bf16[16,2,2048]{2,1,0:T(2,128)(2,1)S(1)}, u32[]{:S(2)}, u32[]{:S(2)}) async-start(bf16[16,2,2048]{2,1,0:T(2,128)(2,1)} %reshape.85), calls=%async_computation.1 | async-start | bytes 262144 | tf_op jit(solution)/shard_map/all_to_all | solution.py:162
  73.6 36.3 %copy-start.4 = (bf16[1,2048,896]{2,1,0:T(8,128)(2,1)S(1)}, bf16[1,2048,896]{2,1,0:T(8,128)(2,1)}, u32[]{:S(2)}) copy-start(bf16[1,2048,896]{2,1,0:T(8,128)(2,1)} %param.28) | copy-start | bytes 11010052
  109.9 4.5 %copy-start.5 = (bf16[1,2048,896]{2,1,0:T(8,128)(2,1)S(1)}, bf16[1,2048,896]{2,1,0:T(8,128)(2,1)}, u32[]{:S(2)}) copy-start(bf16[1,2048,896]{2,1,0:T(8,128)(2,1)} %param.27) | copy-start | bytes 11010052
  114.4 4.8 %copy-start.6 = (bf16[1,896,2048]{2,1,0:T(8,128)(2,1)S(1)}, bf16[1,896,2048]{2,1,0:T(8,128)(2,1)}, u32[]{:S(2)}) copy-start(bf16[1,896,2048]{2,1,0:T(8,128)(2,1)} %param.29) | copy-start | bytes 11010052
  123.9 38.1 %copy-start.3 = (f32[64,2]{0,1:T(2,128)S(1)}, f32[64,2]{0,1:T(2,128)}, u32[]{:S(2)}) copy-start(f32[64,2]{0,1:T(2,128)} %param.26) | copy-start | bytes 1540

commit v3 on v2

--- a/solution.py
+++ b/solution.py
@@ -29,6 +29,11 @@
 
 
 def dot3(a, b, dims=NN):
+    if dims is NN:
+        wide = jnp.concatenate(b, axis=1)
+        both = dot1(jnp.concatenate(a, axis=1), jnp.concatenate((wide, wide), axis=0))
+        half = both.shape[1] // 2
+        return both[:, :half] + both[:, half:]
     return dot1(a[0], b[0], dims) + (dot1(a[0], b[1], dims) + dot1(a[1], b[0], dims))
 
 

time: 164 us -> 164 us (level)
  no operation moved by 1% of the time
where the time goes in v3:
time: 164 us; the launch traced here: 163 us
  Pallas kernels  104 us (63%)
  matrix products  19.9 us (12%)
  waiting for transfers between devices  14 us (9%)
  starting transfers between devices  11.9 us (7%)
  local copies, waits for them, and re-layouts  5.91 us (4%)
  blocking collectives  4.98 us (3%)
  other arithmetic  1.97 us (1%)
    pallas_call x1, Pallas kernels, give_back(): pl.pallas_call(give_back_kernel, out_shape=jax.ShapeDtypeStruct(block, pa...  38.1 us
    pallas_call x1, Pallas kernels, dispatch(): pl.pallas_call(dispatch_kernel, out_shape=jax.ShapeDtypeStruct((groups, 2...  35.8 us
    pallas_call x1, Pallas kernels, mix_here(): pl.pallas_call(mixer_kernel, grid=(width // lanes,), in_specs=[block] * 6...  21.3 us
    all_to_all x1, starting transfers between devices, entering_state(): mine = lax.all_to_all(pairs, axis, split_axis=0, concat_axis=0, tiled=True)  8.35 us
    all_to_all x1, waiting for transfers between devices, entering_state(): back = lax.all_to_all(states, axis, split_axis=0, concat_axis=0, tiled=True)  7.68 us
    all_to_all x1, waiting for transfers between devices, entering_state(): mine = lax.all_to_all(pairs, axis, split_axis=0, concat_axis=0, tiled=True)  6.33 us
    pallas_call x1, Pallas kernels, finish(): pl.pallas_call(finish_kernel, out_shape=jax.ShapeDtypeStruct(local_read.s...  5.11 us
    dot_general x1, matrix products, local(): jnp.dot(gathered, out_weight, preferred_element_type=jnp.float32)  5.09 us
  transfers between devices with their start and end apart: 2, of which 2 were waited for; matrix products, arithmetic and copies ran while one was open for 2% of the time, Pallas kernels for 0%

profile of v3, /device:TPU:0, one launch (start us, length us, event | category | flops | bytes accessed | tf_op | source)
XLA Modules:
  0.0 162.8 jit_solution(12034890070798992702)
XLA Ops:
  0.0 0.0 copy-start.2
  0.0 0.0 copy-start.1
  0.0 21.3 %shard_map.145 = (f32[128,1024]{1,0:T(8,128)}, bf16[128,1024]{1,0:T(8,128)(2,1)}, bf16[16,64,128]{2,1,0:T(8,128)(2,1)}) custom-call(bf16[128,1024]{1,0:T(8,128)(2,1)} %q_ref.1, bf16[128,1024]{1,0:T(8,128)(2,1)} %k_ref.1, bf16[128,1024]{1,0:T(8,128)(2,1)} %v_ref.1, bf16[128,1024]{1,0:T(8,128)(2,1)} %r_ref.1, bf16[128,1024]{1,0:T(8,128)(2,1)} %l_ref.1, ...), custom_call_target="tpu_custom_call" | custom-call | tf_op jit(solution)/shard_map/pallas_call | solution.py:127
  21.3 8.3 %all-to-all-start = ((bf16[16,64,128]{2,1,0:T(8,128)(2,1)}), bf16[16,64,128]{2,1,0:T(8,128)(2,1)S(1)}, u32[]{:S(2)}, u32[]{:S(2)}) async-start(bf16[16,64,128]{2,1,0:T(8,128)(2,1)} %get-tuple-element.10), calls=%async_computation | async-start | bytes 524288 | tf_op jit(solution)/shard_map/all_to_all | solution.py:159
  29.7 1.3 broadcast_in_dim.2.gain_ref
  31.0 0.7 convert_element_type.34
  31.7 0.8 copy.37
  32.4 0.1 eq.58
  32.6 0.1 fusion.15
  32.7 0.2 reduce_window_sum.11
  32.8 0.2 select_reduce_fusion
  33.0 0.1 sub.7
  33.2 0.1 copy.38
  33.2 6.3 %all-to-all-done.pair_ref = bf16[16,64,128]{2,1,0:T(8,128)(2,1)S(1)} async-done(((bf16[16,64,128]{2,1,0:T(8,128)(2,1)}), bf16[16,64,128]{2,1,0:T(8,128)(2,1)S(1)}, u32[]{:S(2)}, u32[]{:S(2)}) %all-to-all-start) | async-done | bytes 262176 | tf_op jit(solution)/shard_map/all_to_all | solution.py:159
  39.6 0.0 copy-start
  39.6 0.7 copy-done
  40.3 3.6 %shard_map.146 = bf16[16,64,64]{2,1,0:T(8,128)(2,1)} custom-call(bf16[16,64,128]{2,1,0:T(8,128)(2,1)} %copy-done), custom_call_target="tpu_custom_call" | custom-call | tf_op jit(solution)/shard_map/pallas_call | solution.py:160
  43.9 1.8 %reshape.85 = bf16[16,2,2048]{2,1,0:T(2,128)(2,1)} reshape(bf16[16,64,64]{2,1,0:T(8,128)(2,1)} %shard_map.146) | data formatting | bytes 262144
  45.8 3.5 %all-to-all-start.1 = ((bf16[16,2,2048]{2,1,0:T(2,128)(2,1)}), bf16[16,2,2048]{2,1,0:T(2,128)(2,1)S(1)}, u32[]{:S(2)}, u32[]{:S(2)}) async-start(bf16[16,2,2048]{2,1,0:T(2,128)(2,1)} %reshape.85), calls=%async_computation.1 | async-start | bytes 262144 | tf_op jit(solution)/shard_map/all_to_all | solution.py:167
  49.3 0.0 copy-done.2
  49.3 0.1 fusion.13
  49.4 7.7 %all-to-all-done.1 = bf16[16,2,2048]{2,1,0:T(2,128)(2,1)S(1)} async-done(((bf16[16,2,2048]{2,1,0:T(2,128)(2,1)}), bf16[16,2,2048]{2,1,0:T(2,128)(2,1)S(1)}, u32[]{:S(2)}, u32[]{:S(2)}) %all-to-all-start.1) | async-done | bytes 131104 | tf_op jit(solution)/shard_map/all_to_all | solution.py:167
  57.1 0.9 reshape.86.state_ref
  58.0 5.1 %shard_map.147 = bf16[128,1024]{1,0:T(8,128)(2,1)} custom-call(f32[128,1024]{1,0:T(8,128)} %get-tuple-element.8.local_ref, bf16[128,1024]{1,0:T(8,128)(2,1)} %get-tuple-element.9.carry_ref, bf16[16,64,64]{2,1,0:T(8,128)(2,1)} %reshape.86.state_ref, bf16[1,1024]{1,0:T(2,128)(2,1)} %broadcast_in_dim.2.gain_ref), custom_call_target="tpu_custom_call" | custom-call | tf_op jit(solution)/shard_map/pallas_call | solution.py:184
  63.1 5.0 %all_to_all.29 = bf16[2,64,1024]{2,1,0:T(8,128)(2,1)S(1)} all-to-all(bf16[2,64,1024]{2,1,0:T(8,128)(2,1)} %bitcast.37), channel_id=1, replica_groups=mesh['sp'=16,'tp'=2] {'tp'}, dimensions={0} | all-to-all | bytes 524288 | tf_op jit(solution)/shard_map/all_to_all | solution.py:385
  68.1 0.0 copy-done.1
  68.1 5.1 %multiply_reduce_fusion = (f32[64]{0:T(128)S(1)}, f32[64,2048]{1,0:T(8,128)S(1)}) fusion(bf16[64,2048]{1,0:T(8,128)(2,1)S(1)} %bitcast.36, bf16[2048,2048]{1,0:T(8,128)(2,1)} %param.23, bf16[64,2048]{1,0:T(8,128)(2,1)S(1)} %copy-done.1), kind=kOutput, calls=%fused_computation.13 | convolution fusion | flops 537395136 | bytes 9437440 | tf_op jit(solution)/shard_map/dot_general | solution.py:386
  73.2 0.0 copy-start.4
  73.3 0.5 convolution_convert_fusion.1
  73.8 35.8 %shard_map.148 = bf16[8,2,2,32,2048]{4,3,2,1,0:T(8,128)(2,1)S(1)} custom-call(bf16[8,32,2048]{2,1,0:T(8,128)(2,1)S(1)} %bitcast.34), custom_call_target="tpu_custom_call" | custom-call | tf_op jit(solution)/shard_map/pallas_call | solution.py:269
  109.6 0.0 copy-done.4
  109.6 0.0 copy-start.5
  109.6 4.5 %fusion.1 = f32[1024,896]{1,0:T(8,128)S(1)} fusion(bf16[1024,2048]{1,0:T(8,128)(2,1)S(1)} %bitcast.31, bf16[1,2048,896]{2,1,0:T(8,128)(2,1)S(1)} %copy-done.4), kind=kOutput, calls=%fused_computation.2 | convolution fusion | flops 3758096384 | bytes 11534336 | tf_op jit(solution)/shard_map/dot_general | solution.py:411
  114.1 0.0 copy-done.5
  114.1 0.0 copy-start.6
  114.1 4.7 %multiply_convert_fusion = bf16[1024,896]{1,0:T(8,128)(2,1)S(1)} fusion(f32[1024,896]{1,0:T(8,128)S(1)} %fusion.1, bf16[1024,2048]{1,0:T(8,128)(2,1)S(1)} %bitcast.32, bf16[1,2048,896]{2,1,0:T(8,128)(2,1)S(1)} %copy-done.5), kind=kOutput, calls=%fused_computation.6 | convolution fusion | flops 3763601408 | bytes 13369344 | tf_op jit(solution)/shard_map/dot_general | solution.py:410
  118.9 0.0 copy-done.6
  118.9 4.7 %convolution_convert_fusion = bf16[1024,2048]{1,0:T(8,128)(2,1)S(1)} fusion(bf16[1024,896]{1,0:T(8,128)(2,1)S(1)} %multiply_convert_fusion, bf16[1,896,2048]{2,1,0:T(8,128)(2,1)S(1)} %copy-done.6), kind=kOutput, calls=%fused_computation | convolution fusion | flops 3760193536 | bytes 9699328 | tf_op jit(solution)/shard_map/dot_general | solution.py:413
  123.6 0.0 copy-start.3
  123.6 38.1 %shard_map.149 = bf16[8,32,2048]{2,1,0:T(8,128)(2,1)S(1)} custom-call(bf16[8,2,2,32,2048]{4,3,2,1,0:T(8,128)(2,1)S(1)} %bitcast.33), custom_call_target="tpu_custom_call" | custom-call | tf_op jit(solution)/shard_map/pallas_call | solution.py:344
  161.7 0.0 copy-done.3
  161.7 0.4 fusion.7
  162.1 0.8 add_convert_fusion
  (4 shorter events, 0.0 us)
Async XLA Ops:
  0.0 49.3 %copy-start.2 = (s32[64,2]{0,1:T(2,128)S(1)}, s32[64,2]{0,1:T(2,128)}, u32[]{:S(2)}) copy-start(s32[64,2]{0,1:T(2,128)} %param.25) | copy-start | bytes 1540
  0.0 68.1 %copy-start.1 = (bf16[64,2048]{1,0:T(8,128)(2,1)S(1)}, bf16[64,2048]{1,0:T(8,128)(2,1)}, u32[]{:S(2)}) copy-start(bf16[64,2048]{1,0:T(8,128)(2,1)} %param.15) | copy-start | bytes 786436
  21.3 18.2 %all-to-all-start = ((bf16[16,64,128]{2,1,0:T(8,128)(2,1)}), bf16[16,64,128]{2,1,0:T(8,128)(2,1)S(1)}, u32[]{:S(2)}, u32[]{:S(2)}) async-start(bf16[16,64,128]{2,1,0:T(8,128)(2,1)} %get-tuple-element.10), calls=%async_computation | async-start | bytes 524288 | tf_op jit(solution)/shard_map/all_to_all | solution.py:159
  39.6 0.7 copy-start
  45.8 11.3 %all-to-all-start.1 = ((bf16[16,2,2048]{2,1,0:T(2,128)(2,1)}), bf16[16,2,2048]{2,1,0:T(2,128)(2,1)S(1)}, u32[]{:S(2)}, u32[]{:S(2)}) async-start(bf16[16,2,2048]{2,1,0:T(2,128)(2,1)} %reshape.85), calls=%async_computation.1 | async-start | bytes 262144 | tf_op jit(solution)/shard_map/all_to_all | solution.py:167
  73.2 36.3 %copy-start.4 = (bf16[1,2048,896]{2,1,0:T(8,128)(2,1)S(1)}, bf16[1,2048,896]{2,1,0:T(8,128)(2,1)}, u32[]{:S(2)}) copy-start(bf16[1,2048,896]{2,1,0:T(8,128)(2,1)} %param.28) | copy-start | bytes 11010052
  109.6 4.5 %copy-start.5 = (bf16[1,2048,896]{2,1,0:T(8,128)(2,1)S(1)}, bf16[1,2048,896]{2,1,0:T(8,128)(2,1)}, u32[]{:S(2)}) copy-start(bf16[1,2048,896]{2,1,0:T(8,128)(2,1)} %param.27) | copy-start | bytes 11010052
  114.1 4.8 %copy-start.6 = (bf16[1,896,2048]{2,1,0:T(8,128)(2,1)S(1)}, bf16[1,896,2048]{2,1,0:T(8,128)(2,1)}, u32[]{:S(2)}) copy-start(bf16[1,896,2048]{2,1,0:T(8,128)(2,1)} %param.29) | copy-start | bytes 11010052
  123.6 38.1 %copy-start.3 = (f32[64,2]{0,1:T(2,128)S(1)}, f32[64,2]{0,1:T(2,128)}, u32[]{:S(2)}) copy-start(f32[64,2]{0,1:T(2,128)} %param.26) | copy-start | bytes 1540
